TPU v7x, 128 devices: a whole 4x4x4 slice. The times are simulated.
128 devices in a mesh: sp: 32 (over z, y, core), tp: 4 (over x).
Axes of the slice: x: 4, y: 4, z: 4, core: 2. Of those that a mesh axis runs over, the one named last changes fastest.
Arguments:
- residual_entry_input: bfloat16 [32768, 2048], P(('sp', 'tp')), may hold values from -6 to 6
- query_matrix_rows: bfloat16 [32768, 1024], P('sp', 'tp'), may hold values from -6 to 6
- key_matrix_rows: bfloat16 [32768, 1024], P('sp', 'tp'), may hold values from -6 to 6
- value_matrix_rows: bfloat16 [32768, 2048], P('sp', 'tp'), may hold values from -6 to 6
- output_gate_logits: bfloat16 [32768, 2048], P('sp', 'tp'), may hold values from -6 to 6
- input_gate_logits: float32 [32768, 8], P('sp', 'tp'), may hold values from -6 to 6
- forget_gate_logits: float32 [32768, 8], P('sp', 'tp'), may hold values from -8 to 31
- forget_decay_offset: float32 [32768, 8], P('sp', 'tp'), may hold values from -0.7 to 0
- head_norm_gain: float32 [8, 256], P('tp'), may hold values from 0.1 to 1.9
- cell_output_weight: bfloat16 [2048, 2048], P('tp'), may hold values from -0.125 to 0.125
- feedforward_norm_gain: float32 [2048], replicated, may hold values from 0.1 to 1.9
- gate_up_weight: bfloat16 [2048, 5632], P('sp', 'tp'), may hold values from -0.125 to 0.125
- value_up_weight: bfloat16 [2048, 5632], P('sp', 'tp'), may hold values from -0.125 to 0.125
- gate_filter_taps: float32 [3, 5632], P(None, 'tp'), may hold values from -3 to 3
- value_filter_taps: float32 [3, 5632], P(None, 'tp'), may hold values from -3 to 3
- down_projection_weight: bfloat16 [5632, 2048], P('tp', 'sp'), may hold values from -0.078125 to 0.078125
Outputs:
- result: bfloat16 [32768, 2048], P(('sp', 'tp'))
All inputs are finite; a program needn't handle non-finite values.
Results may differ from a plain program's by a relative error of at most 0.025.
Values may be sent and summed in bfloat16 or wider, within the bound.
A program may use at most 128 MiB of HBM per device.

v0:
```python
import jax
import jax.numpy as jnp
from jax import lax
from jax.sharding import Mesh
from jax.sharding import PartitionSpec as P

BLOCK = 128
SP = ("sp_0", "sp_1", "sp_2")
SP_TP = ("sp_0", "sp_1", "sp_2", "tp")


eps = 1e-06
neg_large = -1e30


def neutral_like(x, identity):
    return jax.tree.map(
        lambda part, zero: jnp.zeros_like(part) + jnp.asarray(zero, part.dtype), x, identity
    )


def gathered_once(x, axis):
    leaves = jax.tree.leaves(x)
    sequence = sorted(range(len(leaves)), key=lambda k: -leaves[k].size)
    width = (1, *leaves[sequence[0]].shape)[-1]
    lines = [
        jnp.pad(leaves[k].reshape(-1), (0, -leaves[k].size % width)).reshape(-1, width)
        for k in sequence
    ]
    both, at, found = (lax.all_gather(jnp.concatenate(lines), axis), 0, {})
    for k, line in zip(sequence, lines):
        slab = both[:, at : at + len(line)].reshape(len(both), -1)
        found[k] = slab[:, : leaves[k].size].reshape(-1, *leaves[k].shape)
        at += len(line)
    numbers = iter(range(len(leaves)))
    return jax.tree.map(lambda _: found[next(numbers)], x)


def entering(x, axes, combine, identity):
    before = start = neutral_like(x, identity)
    running = x
    for axis in reversed(axes):
        count, position = (lax.axis_size(axis), lax.axis_index(axis))
        pieces = gathered_once(
            jax.tree.map(
                lambda part, kind: part.astype(kind),
                running,
                (jnp.bfloat16, jnp.bfloat16, jnp.bfloat16, jnp.bfloat16),
            ),
            axis,
        )
        inside, running = (start, start)
        for k in range(count):
            passed = k < position
            running = combine(
                running, jax.tree.map(lambda part, own: part[k].astype(own.dtype), pieces, x)
            )
            inside = jax.tree.map(lambda new, old: jnp.where(passed, new, old), running, inside)
        before = combine(inside, before)
    return before


def shifted(x, axis, by):
    count = lax.axis_size(axis)
    pairs = [(i, i + by) for i in range(count) if 0 <= i + by < count]
    return lax.ppermute(x, axis, pairs)


def side_by_side(arrays, axis, dim, along):
    both = jnp.concatenate(arrays, axis=along)
    result, at, finished = (lax.all_gather(both, axis, axis=dim, tiled=True), 0, [])
    for a in arrays:
        finished.append(lax.slice_in_dim(result, at, at + a.shape[along], axis=along))
        at += a.shape[along]
    return tuple(finished)


def laid_out(tiles, dim):
    shape = list(tiles.shape[1:])
    shape[dim] *= tiles.shape[0]
    return jnp.moveaxis(tiles, 0, dim).reshape(shape)


def all_blocks(x, axes, sequence):
    tiles = x
    for k in sequence:
        tiles = lax.all_gather(tiles, axes[k])
    done = sequence[::-1]
    back = [done.index(k) for k in range(len(axes))]
    tiles = tiles.transpose(*back, *range(len(axes), tiles.ndim))
    return tiles.reshape(-1, *x.shape)


def gather_axes(x, axes, sequence, dim):
    return laid_out(all_blocks(x, axes, sequence), dim)


def gate_log_values(input_gate_logits, forget_gate_logits, forget_decay_offset):
    input_log_value = 15.0 * jnp.tanh(input_gate_logits / 15.0)
    forget_log_sigmoid = (
        jax.nn.log_sigmoid(15.0 * jnp.tanh(forget_gate_logits / 15.0)) + forget_decay_offset
    )
    return (input_log_value, forget_log_sigmoid)


def combine_states(earlier, later):
    total_one, memory_one, normer_one, running_one = earlier
    total_two, memory_two, normer_two, running_two = later
    joined = jnp.maximum(total_two + running_one, running_two)
    weight_one = jnp.exp(total_two + running_one - joined)
    weight_two = jnp.exp(running_two - joined)
    memory = weight_one[:, None, None] * memory_one + weight_two[:, None, None] * memory_two
    normer = weight_one[:, None] * normer_one + weight_two[:, None] * normer_two
    return (total_one + total_two, memory, normer, joined)


def local_step(state_carry, inputs):
    memory, normer, running = state_carry
    query_block, key_block, value_block, input_block, forget_block = inputs
    length = query_block.shape[0]
    highest = lax.Precision.DEFAULT
    query_scale = query_block.shape[2] ** (-0.5)
    causal = jnp.tril(jnp.ones((length, length), dtype=bool))[:, :, None]
    cumulative = jnp.cumsum(forget_block, axis=0)
    logits = cumulative[:, None, :] - cumulative[None, :, :] + input_block[None, :, :]
    logits = jnp.where(causal, logits, -jnp.inf)
    carried = cumulative + running[None, :]
    stable = jnp.maximum(carried, jnp.max(logits, axis=1))
    carry_weight = jnp.exp(carried - stable)
    raw = (
        jnp.einsum("thd,shd->tsh", query_block, key_block, preferred_element_type=jnp.float32)
        * query_scale
    )
    scores = raw * jnp.exp(logits - stable[:, None, :])
    scaled_query = query_block.astype(jnp.float32) * query_scale
    numerator = carry_weight[:, :, None] * jnp.einsum(
        "hvd,thd->thv", memory, scaled_query, precision=highest
    )
    numerator = numerator + jnp.einsum(
        "tsh,shv->thv", scores.astype(jnp.bfloat16), value_block, preferred_element_type=jnp.float32
    )
    denominator = carry_weight * jnp.einsum(
        "hd,thd->th", normer, scaled_query, precision=highest
    ) + jnp.sum(scores, axis=1)
    last_sum = cumulative[-1]
    weights_log = last_sum[None, :] - cumulative + input_block
    new_running = jnp.maximum(last_sum + running, jnp.max(weights_log, axis=0))
    decay_factor = jnp.exp(last_sum + running - new_running)
    weighted = (
        key_block.astype(jnp.float32) * jnp.exp(weights_log - new_running[None, :])[:, :, None]
    )
    memory = decay_factor[:, None, None] * memory + jnp.einsum(
        "shv,shd->hvd",
        value_block,
        weighted.astype(jnp.bfloat16),
        preferred_element_type=jnp.float32,
    )
    normer = decay_factor[:, None] * normer + jnp.sum(weighted, axis=0)
    return ((memory, normer, new_running), (numerator, denominator, stable))


def local(
    residual_entry_input,
    query_matrix_rows,
    key_matrix_rows,
    value_matrix_rows,
    output_gate_logits,
    input_gate_logits,
    forget_gate_logits,
    forget_decay_offset,
    head_norm_gain,
    cell_output_weight,
    feedforward_norm_gain,
    gate_up_weight,
    value_up_weight,
    gate_filter_taps,
    value_filter_taps,
    down_projection_weight,
):
    highest = lax.Precision.DEFAULT
    token_count = query_matrix_rows.shape[0]
    head_count = input_gate_logits.shape[1]
    key_width = query_matrix_rows.shape[1] // head_count
    value_width = value_matrix_rows.shape[1] // head_count
    query_scale = key_width ** (-0.5)
    queries_low = query_matrix_rows.reshape(token_count, head_count, key_width)
    keys_low = key_matrix_rows.reshape(token_count, head_count, key_width)
    values_low = value_matrix_rows.reshape(token_count, head_count, value_width)
    input_log_value, forget_log_sigmoid = gate_log_values(
        input_gate_logits, forget_gate_logits, forget_decay_offset
    )
    cumulative = jnp.cumsum(forget_log_sigmoid, axis=0)
    total_log = cumulative[-1]
    block_count = token_count // BLOCK

    def blocks(tensor):
        return tensor.reshape((block_count, BLOCK) + tensor.shape[1:])

    initial = (
        jnp.zeros((head_count, value_width, key_width), jnp.float32),
        jnp.zeros((head_count, key_width), jnp.float32),
        jnp.full((head_count,), neg_large, jnp.float32),
    )
    end_state, (numerator, denominator, stable) = lax.scan(
        local_step,
        initial,
        (
            blocks(queries_low),
            blocks(keys_low),
            blocks(values_low),
            blocks(input_log_value),
            blocks(forget_log_sigmoid),
        ),
    )
    end_memory, end_normer, end_running = end_state
    identity = (
        jnp.zeros((head_count,), jnp.float32),
        jnp.zeros((head_count, value_width, key_width), jnp.float32),
        jnp.zeros((head_count, key_width), jnp.float32),
        jnp.full((head_count,), neg_large, jnp.float32),
    )
    prefix = entering(
        (total_log, end_memory, end_normer, end_running), SP, combine_states, identity
    )
    numerator = numerator.reshape(token_count, head_count, value_width)
    denominator = denominator.reshape(token_count, head_count)
    stable = stable.reshape(token_count, head_count)
    _, prior_memory, prior_normer, prior_running = prefix
    scaled_query = queries_low.astype(jnp.float32) * query_scale
    prior_log = cumulative + prior_running[None, :]
    top_log = jnp.maximum(stable, prior_log)
    local_weight = jnp.exp(stable - top_log)
    prior_weight = jnp.exp(prior_log - top_log)
    numerator = local_weight[:, :, None] * numerator + prior_weight[:, :, None] * jnp.einsum(
        "hvd,thd->thv", prior_memory, scaled_query, precision=highest
    )
    denominator = local_weight * denominator + prior_weight * jnp.einsum(
        "hd,thd->th", prior_normer, scaled_query, precision=highest
    )
    memory_out = numerator / jnp.maximum(jnp.abs(denominator), jnp.exp(-top_log))[:, :, None]
    normed = (
        memory_out
        * lax.rsqrt(jnp.mean(memory_out * memory_out, axis=-1, keepdims=True) + eps)
        * head_norm_gain[None, :, :]
    )
    gated_rows = (
        normed.reshape(token_count, head_count * value_width)
        * jax.nn.sigmoid(output_gate_logits.astype(jnp.float32))
    ).astype(jnp.bfloat16)
    whole_out = lax.all_gather(cell_output_weight, "tp", axis=0, tiled=True)
    own_rows = lax.all_to_all(gated_rows, "tp", split_axis=0, concat_axis=1, tiled=True)
    mixed_rows = jnp.dot(own_rows, whole_out, preferred_element_type=jnp.float32)
    stream_wide = residual_entry_input.astype(jnp.float32) + mixed_rows
    stream = stream_wide.astype(jnp.bfloat16)
    stream_wide = lax.optimization_barrier(stream).astype(jnp.float32)
    normed_rows = (
        stream_wide
        * lax.rsqrt(jnp.mean(stream_wide * stream_wide, axis=-1, keepdims=True) + eps)
        * feedforward_norm_gain[None, :]
    ).astype(jnp.bfloat16)
    group_rows = lax.all_gather(normed_rows, "tp", axis=0, tiled=True)
    earlier_rows = shifted(group_rows[-2:], SP, 1)
    window = jnp.concatenate([earlier_rows, group_rows], axis=0)
    pieces = side_by_side((gate_up_weight, value_up_weight), SP, 0, 1)
    up_gate = jnp.dot(window, pieces[0], preferred_element_type=jnp.float32)
    up_value = jnp.dot(window, pieces[1], preferred_element_type=jnp.float32)
    conv_g = (
        gate_filter_taps[0][None, :] * up_gate[:-2]
        + gate_filter_taps[1][None, :] * up_gate[1:-1]
        + gate_filter_taps[2][None, :] * up_gate[2:]
    )
    conv_v = (
        value_filter_taps[0][None, :] * up_value[:-2]
        + value_filter_taps[1][None, :] * up_value[1:-1]
        + value_filter_taps[2][None, :] * up_value[2:]
    )
    hidden = (jax.nn.silu(conv_g) * conv_v).astype(jnp.bfloat16)
    whole_down = gather_axes(down_projection_weight, (("sp_0", "sp_1"), "sp_2"), (0, 1), 1)
    ffn_rows = lax.psum_scatter(
        jnp.dot(hidden, whole_down, preferred_element_type=jnp.float32).astype(jnp.bfloat16),
        "tp",
        scatter_dimension=0,
        tiled=True,
    ).astype(jnp.float32)
    return (stream_wide + ffn_rows).astype(jnp.bfloat16)


def solution(mesh):
    split = Mesh(mesh.devices.reshape(4, 4, 2, mesh.shape["tp"]), ("sp_0", "sp_1", "sp_2", "tp"))
    placed = (
        P(SP_TP, None),
        P(SP, "tp"),
        P(SP, "tp"),
        P(SP, "tp"),
        P(SP, "tp"),
        P(SP, "tp"),
        P(SP, "tp"),
        P(SP, "tp"),
        P("tp", None),
        P("tp", None),
        P(),
        P(SP, "tp"),
        P(SP, "tp"),
        P(None, "tp"),
        P(None, "tp"),
        P("tp", SP),
    )
    return jax.shard_map(
        local, mesh=split, in_specs=placed, out_specs=P(SP_TP, None), check_vma=False
    )
```

profile of v0, /device:TPU:0, one launch (start us, length us, event | category | flops | bytes accessed | tf_op | source)
XLA Modules:
  0.0 418.4 jit_solution(10256180526580571442)
XLA Ops:
  6.5 0.7 all-gather.14.cloned.1.call-update
  7.3 0.7 all-gather.20.cloned.1.call-update
  8.1 0.7 fusion.147
  9.1 1.3 reshape.1706
  10.7 0.9 reshape.1707
  11.7 2.0 reshape.1708
  13.6 102.5 %while.21 = (s32[]{:T(128)}, f32[2,256,128]{2,1,0:T(8,128)S(1)}, f32[2,128]{1,0:T(2,128)S(1)}, f32[2]{0:T(128)S(1)}, f32[8,128,2,256]{1,0,3,2:T(8,128)}, /*index...) while((s32[]{:T(128)}, f32[2,256,128]{2,1,0:T(8,128)S(1)}, ...), condition=%wide.region_6.7_spmd.clone, body=%wide.region_0.6_spmd.clone.sunk | while | flops 59952648 | bytes 4685610 | solution.py:204
  14.4 1.0 constant_dynamic-slice_fusion.6
  17.8 8.3 %dynamic_update_slice.19 = f32[8,128,2,256]{1,0,3,2:T(8,128)} dynamic-update-slice(f32[8,128,2,256]{1,0,3,2:T(8,128)} %get-tuple-element.428, f32[1,128,2,256]{1,0,3,2:T(1,128)S(1)} %copy.336, s32[]{:T(128)} %get-tuple-element.424, s32[]{:T(128)} %constant.38.clone.1..sunk, s32[]{:T(128)} %constant.38.clone.1..sunk, s32[]{:T(128)} %constant.38.clone.1..sunk) | dynamic-update-slice | bytes 524292 | tf_op jit(solution)/shard_map/while/body/jit(dynamic_update_index_in_dim)/dynamic_update_slice | solution.py:204
  27.3 1.0 constant_dynamic-slice_fusion.6
  30.7 8.2 %dynamic_update_slice.19 = f32[8,128,2,256]{1,0,3,2:T(8,128)} dynamic-update-slice(f32[8,128,2,256]{1,0,3,2:T(8,128)} %get-tuple-element.428, f32[1,128,2,256]{1,0,3,2:T(1,128)S(1)} %copy.336, s32[]{:T(128)} %get-tuple-element.424, s32[]{:T(128)} %constant.38.clone.1..sunk, s32[]{:T(128)} %constant.38.clone.1..sunk, s32[]{:T(128)} %constant.38.clone.1..sunk) | dynamic-update-slice | bytes 524292 | tf_op jit(solution)/shard_map/while/body/jit(dynamic_update_index_in_dim)/dynamic_update_slice | solution.py:204
  40.1 1.0 constant_dynamic-slice_fusion.6
  43.5 8.2 %dynamic_update_slice.19 = f32[8,128,2,256]{1,0,3,2:T(8,128)} dynamic-update-slice(f32[8,128,2,256]{1,0,3,2:T(8,128)} %get-tuple-element.428, f32[1,128,2,256]{1,0,3,2:T(1,128)S(1)} %copy.336, s32[]{:T(128)} %get-tuple-element.424, s32[]{:T(128)} %constant.38.clone.1..sunk, s32[]{:T(128)} %constant.38.clone.1..sunk, s32[]{:T(128)} %constant.38.clone.1..sunk) | dynamic-update-slice | bytes 524292 | tf_op jit(solution)/shard_map/while/body/jit(dynamic_update_index_in_dim)/dynamic_update_slice | solution.py:204
  52.9 1.0 constant_dynamic-slice_fusion.6
  56.3 8.2 %dynamic_update_slice.19 = f32[8,128,2,256]{1,0,3,2:T(8,128)} dynamic-update-slice(f32[8,128,2,256]{1,0,3,2:T(8,128)} %get-tuple-element.428, f32[1,128,2,256]{1,0,3,2:T(1,128)S(1)} %copy.336, s32[]{:T(128)} %get-tuple-element.424, s32[]{:T(128)} %constant.38.clone.1..sunk, s32[]{:T(128)} %constant.38.clone.1..sunk, s32[]{:T(128)} %constant.38.clone.1..sunk) | dynamic-update-slice | bytes 524292 | tf_op jit(solution)/shard_map/while/body/jit(dynamic_update_index_in_dim)/dynamic_update_slice | solution.py:204
  65.7 1.0 constant_dynamic-slice_fusion.6
  69.1 8.2 %dynamic_update_slice.19 = f32[8,128,2,256]{1,0,3,2:T(8,128)} dynamic-update-slice(f32[8,128,2,256]{1,0,3,2:T(8,128)} %get-tuple-element.428, f32[1,128,2,256]{1,0,3,2:T(1,128)S(1)} %copy.336, s32[]{:T(128)} %get-tuple-element.424, s32[]{:T(128)} %constant.38.clone.1..sunk, s32[]{:T(128)} %constant.38.clone.1..sunk, s32[]{:T(128)} %constant.38.clone.1..sunk) | dynamic-update-slice | bytes 524292 | tf_op jit(solution)/shard_map/while/body/jit(dynamic_update_index_in_dim)/dynamic_update_slice | solution.py:204
  78.5 1.0 constant_dynamic-slice_fusion.6
  81.9 8.2 %dynamic_update_slice.19 = f32[8,128,2,256]{1,0,3,2:T(8,128)} dynamic-update-slice(f32[8,128,2,256]{1,0,3,2:T(8,128)} %get-tuple-element.428, f32[1,128,2,256]{1,0,3,2:T(1,128)S(1)} %copy.336, s32[]{:T(128)} %get-tuple-element.424, s32[]{:T(128)} %constant.38.clone.1..sunk, s32[]{:T(128)} %constant.38.clone.1..sunk, s32[]{:T(128)} %constant.38.clone.1..sunk) | dynamic-update-slice | bytes 524292 | tf_op jit(solution)/shard_map/while/body/jit(dynamic_update_index_in_dim)/dynamic_update_slice | solution.py:204
  91.3 1.0 constant_dynamic-slice_fusion.6
  94.7 8.2 %dynamic_update_slice.19 = f32[8,128,2,256]{1,0,3,2:T(8,128)} dynamic-update-slice(f32[8,128,2,256]{1,0,3,2:T(8,128)} %get-tuple-element.428, f32[1,128,2,256]{1,0,3,2:T(1,128)S(1)} %copy.336, s32[]{:T(128)} %get-tuple-element.424, s32[]{:T(128)} %constant.38.clone.1..sunk, s32[]{:T(128)} %constant.38.clone.1..sunk, s32[]{:T(128)} %constant.38.clone.1..sunk) | dynamic-update-slice | bytes 524292 | tf_op jit(solution)/shard_map/while/body/jit(dynamic_update_index_in_dim)/dynamic_update_slice | solution.py:204
  104.1 1.0 constant_dynamic-slice_fusion.6
  107.5 8.2 %dynamic_update_slice.19 = f32[8,128,2,256]{1,0,3,2:T(8,128)} dynamic-update-slice(f32[8,128,2,256]{1,0,3,2:T(8,128)} %get-tuple-element.428, f32[1,128,2,256]{1,0,3,2:T(1,128)S(1)} %copy.336, s32[]{:T(128)} %get-tuple-element.424, s32[]{:T(128)} %constant.38.clone.1..sunk, s32[]{:T(128)} %constant.38.clone.1..sunk, s32[]{:T(128)} %constant.38.clone.1..sunk) | dynamic-update-slice | bytes 524292 | tf_op jit(solution)/shard_map/while/body/jit(dynamic_update_index_in_dim)/dynamic_update_slice | solution.py:204
  117.4 2.0 all-gather.5
  121.3 15.1 %all-gather.6 = bf16[4,516,128]{2,1,0:T(8,128)(2,1)S(1)} all-gather(bf16[1,516,128]{2,1,0:T(8,128)(2,1)S(1)} %maximum_bitcast_fusion.1), channel_id=3, replica_groups=mesh['sp_0'=4,'sp_1'=4,'sp_2'=2,'tp'=4] {'sp_1'}, dimensions={0}, use_global_device_ids=true | all-gather | bytes 660480 | tf_op jit(solution)/shard_map/all_gather | solution.py:30
  137.9 16.0 %all-gather.7 = bf16[4,516,128]{2,1,0:T(8,128)(2,1)S(1)} all-gather(bf16[1,516,128]{2,1,0:T(8,128)(2,1)S(1)} %maximum_bitcast_fusion.2), channel_id=4, replica_groups=mesh['sp_0'=4,'sp_1'=4,'sp_2'=2,'tp'=4] {'sp_0'}, dimensions={0}, use_global_device_ids=true | all-gather | bytes 660480 | tf_op jit(solution)/shard_map/all_gather | solution.py:30
  154.3 1.7 reshape.1638
  156.1 0.8 fusion.167
  157.1 1.3 fusion.47
  158.7 1.3 multiply_reduce_fusion
  160.2 1.9 copy.197
  162.1 2.5 multiply_convert_fusion
  164.6 15.5 %all_to_all.19 = bf16[4,256,512]{2,1,0:T(8,128)(2,1)S(1)} all-to-all(bf16[4,256,512]{2,1,0:T(8,128)(2,1)S(1)} %bitcast.610), channel_id=1, replica_groups=mesh['sp_0'=4,'sp_1'=4,'sp_2'=2,'tp'=4] {'tp'}, dimensions={0} | all-to-all | bytes 2097152 | tf_op jit(solution)/shard_map/all_to_all | solution.py:251
  180.7 5.7 %fusion.40 = bf16[256,2048]{1,0:T(8,128)(2,1)S(1)} fusion(bf16[256,2048]{0,1:T(8,128)(2,1)S(1)} %bitcast.606, bf16[2048,2048]{1,0:T(8,128)(2,1)} %all-gather.14.cloned.1.call-done, bf16[256,2048]{1,0:T(8,128)(2,1)S(1)} %copy-done), kind=kOutput, calls=%fused_computation.77 | convolution fusion | flops 2149056512 | bytes 11534336 | tf_op jit(solution)/shard_map/dot_general | solution.py:252
  186.8 1.3 fusion.43
  188.2 3.8 copy.246
  192.1 0.8 pad_maximum_fusion.3
  193.0 40.5 %all-gather.16.cloned.1.call-done = bf16[1024,2048]{1,0:T(8,128)(2,1)} async-done(((bf16[256,2048]{1,0:T(8,128)(2,1)}), bf16[1024,2048]{1,0:T(8,128)(2,1)}) %all-gather.16.cloned.1.call-update) | async-done | bytes 4194320 | tf_op jit(solution)/shard_map/all_gather | solution.py:261
  233.5 0.8 slice.352
  234.2 1.8 collective-permute-start
  236.1 17.9 %all-gather.22.cloned.1.call-done = bf16[32,1408,64]{1,0,2:T(8,128)(2,1)} async-done(((bf16[16,1408,64]{1,0,2:T(8,128)(2,1)}), bf16[32,1408,64]{1,0,2:T(8,128)(2,1)}) %all-gather.22.cloned.1.call-update) | async-done | bytes 5767184 | tf_op jit(solution)/shard_map/all_gather | solution.py:87
  254.0 7.0 %copy.200 = bf16[16,2,1408,64]{2,3,1,0:T(8,128)(2,1)} copy(bf16[16,2,1408,64]{2,0,1,3:T(8,128)(2,1)} %bitcast.607) | data formatting | bytes 11534336 | tf_op jit(solution)/shard_map/transpose | solution.py:90
  261.1 56.7 %all-gather.18.cloned.1.call-done = bf16[2048,2816]{1,0:T(8,128)(2,1)} async-done(((bf16[64,2816]{1,0:T(8,128)(2,1)}), bf16[2048,2816]{1,0:T(8,128)(2,1)}) %all-gather.18.cloned.1.call-update) | async-done | bytes 11534352 | tf_op jit(solution)/shard_map/all_gather | solution.py:71
  317.8 11.9 %fusion.37 = f32[1026,1408]{1,0:T(8,128)} fusion(bf16[2048,2816]{1,0:T(8,128)(2,1)} %all-gather.18.cloned.1.call-done, bf16[1024,2048]{1,0:T(8,128)(2,1)} %all-gather.16.cloned.1.call-done, bf16[2,2048]{1,0:T(2,128)(2,1)S(1)} %collective-permute-done), kind=kOutput, calls=%fused_computation.69 | convolution fusion | flops 5925519360 | bytes 15748096 | tf_op jit(solution)/shard_map/dot_general | solution.py:265
  329.8 8.7 %fusion.33 = f32[1026,1408]{1,0:T(8,128)} fusion(bf16[2048,2816]{1,0:T(8,128)(2,1)S(1)} %copy-done.13, bf16[1024,2048]{1,0:T(8,128)(2,1)S(1)} %copy-done.12, bf16[2,2048]{1,0:T(2,128)(2,1)S(1)} %collective-permute-done), kind=kOutput, calls=%fused_computation.62 | convolution fusion | flops 5925519360 | bytes 15748096 | tf_op jit(solution)/shard_map/dot_general | solution.py:266
  338.4 24.1 %convolution_convert_fusion = bf16[1024,2048]{1,0:T(8,128)(2,1)} fusion(bf16[1408,2048]{0,1:T(8,128)(2,1)} %bitcast.608, f32[1026,1408]{1,0:T(8,128)} %fusion.33, f32[1026,1408]{1,0:T(8,128)} %fusion.37, f32[1408]{0:T(1024)S(1)} %get-tuple-element.181, f32[1408]{0:T(1024)S(1)} %get-tuple-element.182, f32[1408]{0:T(1024)S(1)} %get-tuple-element.180, ...), kind=kOutput, calls=%fused_computation.72 | convolution fusion | flops 5930745856 | bytes 44598272 | tf_op jit(solution)/shard_map/dot_general | solution.py:280
  362.6 46.4 %reduce-scatter.2.cloned.1.call-done = bf16[256,2048]{1,0:T(8,128)(2,1)} async-done(((bf16[1024,2048]{1,0:T(8,128)(2,1)}), bf16[256,2048]{1,0:T(8,128)(2,1)}) %reduce-scatter.2.cloned.1.call-update) | async-done | bytes 1048592 | tf_op jit(solution)/shard_map/reduce_scatter | solution.py:279
  409.0 2.6 fusion.44
  (341 shorter events, 35.2 us)
Async XLA Ops:
  6.5 3.9 copy-start.10
  6.5 4.2 %copy-start.1 = (bf16[1024,256]{1,0:T(8,128)(2,1)S(1)}, bf16[1024,256]{1,0:T(8,128)(2,1)}, u32[]{:S(2)}) copy-start(bf16[1024,256]{1,0:T(8,128)(2,1)} %param.20) | copy-start | bytes 1572868
  6.5 174.2 %all-gather.14.cloned.1.call-start = ((), (), s32[]{:S(2)}) async-start(), calls=%async_computation.2 | async-start | bytes 10485760 | tf_op jit(solution)/shard_map/all_gather | solution.py:250
  7.3 180.9 %all-gather.20.cloned.1.call-start = ((), (), s32[]{:S(2)}) async-start(), calls=%async_computation.6 | async-start | bytes 3063808 | tf_op jit(solution)/shard_map/all_gather | solution.py:87
  8.0 225.5 %all-gather.16.cloned.1.call-start = ((), (), s32[]{:S(2)}) async-start(), calls=%async_computation.3 | async-start | bytes 5242880 | tf_op jit(solution)/shard_map/all_gather | solution.py:261
  116.1 37.9 %copy-start.4 = (f32[8,128,2]{2,1,0:T(8,128)S(1)}, f32[8,128,2]{2,1,0:T(8,128)}, u32[]{:S(2)}) copy-start(f32[8,128,2]{2,1,0:T(8,128)} %get-tuple-element.72) | copy-start | bytes 24580
  116.1 38.0 %copy-start.3 = (f32[8,128,2]{2,1,0:T(8,128)S(1)}, f32[8,128,2]{2,1,0:T(8,128)}, u32[]{:S(2)}) copy-start(f32[8,128,2]{2,1,0:T(8,128)} %get-tuple-element.77) | copy-start | bytes 24580
  156.1 2.6 copy-start.2
  158.6 1.3 copy-start.11
  162.1 18.6 %copy-start = (bf16[256,2048]{1,0:T(8,128)(2,1)S(1)}, bf16[256,2048]{1,0:T(8,128)(2,1)}, u32[]{:S(2)}) copy-start(bf16[256,2048]{1,0:T(8,128)(2,1)} %param.18) | copy-start | bytes 3145732
  180.7 6.0 %copy-start.9 = (f32[2048]{0:T(1024)S(1)}, f32[2048]{0:T(1024)}, u32[]{:S(2)}) copy-start(f32[2048]{0:T(1024)} %param.28) | copy-start | bytes 24580
  188.1 66.0 %all-gather.22.cloned.1.call-start = ((), (), s32[]{:S(2)}) async-start(), calls=%async_computation.7 | async-start | bytes 8650752 | tf_op jit(solution)/shard_map/all_gather | solution.py:87
  188.1 4.0 copy-start.5
  188.2 4.0 copy-start.6
  188.2 47.8 %copy-start.7 = (f32[3,1408]{1,0:T(4,128)S(1)}, f32[3,1408]{1,0:T(4,128)}, u32[]{:S(2)}) copy-start(f32[3,1408]{1,0:T(4,128)} %param.32) | copy-start | bytes 50692
  188.2 47.8 %copy-start.8 = (f32[3,1408]{1,0:T(4,128)S(1)}, f32[3,1408]{1,0:T(4,128)}, u32[]{:S(2)}) copy-start(f32[3,1408]{1,0:T(4,128)} %param.31) | copy-start | bytes 50692
  192.1 125.7 %all-gather.18.cloned.1.call-start = ((), (), s32[]{:S(2)}) async-start(), calls=%async_computation.4 | async-start | bytes 11894784 | tf_op jit(solution)/shard_map/all_gather | solution.py:71
  192.9 216.1 %reduce-scatter.2.cloned.1.call-start = ((), (), s32[]{:S(2)}) async-start(), calls=%async_computation.5 | async-start | bytes 5242880 | tf_op jit(solution)/shard_map/reduce_scatter | solution.py:279
  234.2 26.8 %collective-permute-start = (bf16[2,2048]{1,0:T(2,128)(2,1)S(1)}, bf16[2,2048]{1,0:T(2,128)(2,1)S(1)}, u32[]{:S(2)}, u32[]{:S(2)}) collective-permute-start(bf16[2,2048]{1,0:T(2,128)(2,1)S(1)} %slice.352), channel_id=1, source_target_pairs={{0,4},{4,8},{8,12},{12,16},{16,20},{20,24},{24,28},{28,32},{32,36}... | collective-permute-start | bytes 24584 | tf_op jit(solution)/shard_map/ppermute | solution.py:66
  317.8 11.9 %copy-start.12 = (bf16[1024,2048]{1,0:T(8,128)(2,1)S(1)}, bf16[1024,2048]{1,0:T(8,128)(2,1)}, u32[]{:S(2)}) copy-start(bf16[1024,2048]{1,0:T(8,128)(2,1)} %all-gather.16.cloned.1.call-done) | copy-start | bytes 12582916
  317.8 11.9 %copy-start.13 = (bf16[2048,2816]{1,0:T(8,128)(2,1)S(1)}, bf16[2048,2816]{1,0:T(8,128)(2,1)}, u32[]{:S(2)}) copy-start(bf16[2048,2816]{1,0:T(8,128)(2,1)} %all-gather.18.cloned.1.call-done) | copy-start | bytes 34603012
Sparse Core Ops, SparseCore 0:
  9.0 85.5 all-gather.13
  96.8 51.5 all-gather.19
  188.2 45.2 all-gather.15
  235.0 19.0 all-gather.21
  256.1 61.6 all-gather.17
  362.7 46.2 reduce-scatter.1
where the time goes:
time: 421 us; the launch traced here: 418 us
  waiting for transfers between devices  163 us (39%)
  local copies, waits for them, and re-layouts  105 us (25%)
  matrix products  62.1 us (15%)
  blocking collectives  48.7 us (12%)
  other arithmetic  23.2 us (6%)
  between operations  14.1 us (3%)
    dynamic_update_slice x16, local copies, waits for them, and re-layouts, local(): lax.scan(local_step, initial, (blocks(queries_low), blocks(keys_low), blo...  66.9 us
    all_gather x1, waiting for transfers between devices, side_by_side(): lax.all_gather(both, axis, axis=dim, tiled=True)  56.7 us
    reduce_scatter x1, waiting for transfers between devices, local(): lax.psum_scatter(jnp.dot(hidden, whole_down, preferred_element_type=jnp.f...  46.4 us
    all_gather x1, waiting for transfers between devices, local(): group_rows = lax.all_gather(normed_rows, 'tp', axis=0, tiled=True)  40.5 us
    all_gather x3, blocking collectives, gathered_once(): both, at, found = (lax.all_gather(jnp.concatenate(lines), axis), 0, {})  33.1 us
    dot_general x1, matrix products, local(): jnp.dot(hidden, whole_down, preferred_element_type=jnp.float32)  24.1 us
    all_gather x2, waiting for transfers between devices, all_blocks(): tiles = lax.all_gather(tiles, axes[k])  17.9 us
    all_to_all x1, blocking collectives, local(): lax.all_to_all(gated_rows, 'tp', split_axis=0, concat_axis=1, tiled=True)  15.5 us
  transfers between devices with their start and end apart: 7, of which 4 were waited for; matrix products, arithmetic and copies ran while one was open for 34% of the time, Pallas kernels for 0%

commit v1 on v0

v1 whole, which is shorter than its diff:
```python
import jax
import jax.numpy as jnp
from jax import lax
from jax.experimental import pallas as pl
from jax.experimental.pallas import tpu as pltpu
from jax.sharding import Mesh
from jax.sharding import PartitionSpec as P

SP = ("sp_0", "sp_1", "sp_2")
SP_TP = ("sp_0", "sp_1", "sp_2", "tp")
MESH = pl.DeviceIdType.MESH

EPS = 1e-06
NEG = -1e30
L = 128
CH = 8
DK = 128
DV = 256
D = 2048
FFD = 1408
NT = FFD // 128
SCALE = DK**-0.5
F32 = jnp.float32
BF = jnp.bfloat16


def log1p_of(e):
    series = e * (1.0 - e * (0.5 - e * (1.0 / 3.0 - e * (0.25 - e * 0.2))))
    return jnp.where(e < 0.03, series, jnp.log(1.0 + e))


def kernel(
    res, q_in, k_in, v_in, og_in, ig, fg, off, gain, wo_in, fgain, gup, vup, dwn, gtap, vtap,
    out,
    q, k, v, og, rsd, wgv, wd, wo, dc, nl, colt, rows, cs, cpri, mpri, rs_rows,
    st1, ax1, st1r, ax1r, st2, ax2, st3, ax3, st4, ax4, st4r, ax4r,
    gated, orr, stream, gr, hs, hr, hp, hid, ps, rr,
    lsem, ssem, rsem,
):
    z, y, c, tp = (lax.axis_index(a) for a in SP_TP)

    def up(i, n):
        return lax.rem(i + n, 4)

    y1, y3 = up(y, 1), up(y, 3)
    z1, z3 = up(z, 1), up(z, 3)
    x1, x2, x3 = up(tp, 1), up(tp, 2), up(tp, 3)
    other = 1 - c
    place = z * 8 + y * 2 + c

    def at_place(n):
        n = lax.rem(n + 32, 32)
        return {"sp_0": n // 8, "sp_1": lax.rem(n // 2, 4), "sp_2": lax.rem(n, 2)}

    count = {"l": 0, "s": 0, "r": 0}
    open_sends = []

    def take(kind):
        count[kind] += 1
        return count[kind] - 1

    def load(src, dst):
        cp = pltpu.make_async_copy(src, dst, lsem.at[take("l")])
        cp.start()
        return cp

    def send(src, dst, dev):
        cp = pltpu.make_async_remote_copy(
            src_ref=src, dst_ref=dst, send_sem=ssem.at[take("s")], recv_sem=rsem.at[take("r")],
            device_id=dev, device_id_type=MESH,
        )
        cp.start()
        open_sends.append(cp)
        return cp

    def arrived(copies):
        for cp in copies:
            cp.wait_recv()

    ld_k = load(k_in, k)
    ld_v = load(v_in, v)
    ld_w = [load(dwn, wd.at[z, y, c])]
    for n in range(NT):
        ld_w.append(load(gup.at[:, pl.ds(n * 128, 128)], wgv.at[z, y, c, :, pl.ds(n * 256, 128)]))
        ld_w.append(load(vup.at[:, pl.ds(n * 128, 128)], wgv.at[z, y, c, :, pl.ds(n * 256 + 128, 128)]))
    ld_wo = load(wo_in, wo.at[tp])
    ld_q = load(q_in, q)
    ld_og = load(og_in, og)
    ld_res = load(res, rsd)

    barrier = pltpu.get_barrier_semaphore()

    def hello(dev):
        pl.semaphore_signal(barrier, inc=1, device_id=dev, device_id_type=MESH)

    hello({"sp_2": other})
    for n in (1, 2, 3):
        hello({"sp_1": up(y, n)})
        hello({"sp_0": up(z, n)})
        hello({"tp": up(tp, n)})
    hello({**at_place(place - 1), "tp": 3})

    @pl.when(tp == 3)
    def _():
        for t in range(4):
            hello({**at_place(place + 1), "tp": t})
        pl.semaphore_wait(barrier, 15)

    @pl.when(tp != 3)
    def _():
        pl.semaphore_wait(barrier, 11)

    def halves(ref, zz, yy, lo, n):
        return ref.at[zz, yy, c, pl.ds(lo, n)]

    for cp in ld_w:
        cp.wait()
    p1 = []
    for ref in (wgv, wd):
        mine_a, mine_b = halves(ref, z, y, 0, 32), halves(ref, z, y, 32, 32)
        p1 += [
            send(mine_a, mine_a, {"sp_1": y1}),
            send(mine_a, mine_a, {"sp_1": y3}),
            send(mine_b, mine_b, {"sp_0": z1}),
            send(mine_b, mine_b, {"sp_0": z3}),
        ]
    ld_wo.wait()
    wo_half = wo.at[tp, pl.ds(c * 256, 256)]
    w1 = [send(wo_half, wo_half, {"tp": x1}), send(wo_half, wo_half, {"tp": x3})]

    il = 15.0 * jnp.tanh(ig[...] / 15.0)
    xf = 15.0 * jnp.tanh(fg[...] / 15.0)
    fl = jnp.minimum(xf, 0.0) - log1p_of(jnp.exp(-jnp.abs(xf))) + off[...]
    r_i = lax.broadcasted_iota(jnp.int32, (L, L), 0)
    c_i = lax.broadcasted_iota(jnp.int32, (L, L), 1)
    causal = r_i >= c_i
    upper = (r_i <= c_i).astype(F32)
    cum = jnp.dot(fl, upper, preferred_element_type=F32, precision=lax.Precision.HIGHEST)
    a = il - cum
    lane = lax.broadcasted_iota(jnp.int32, (2 * CH, L), 1)
    cm = a
    for s in (1, 2, 4, 8, 16, 32, 64):
        cm = jnp.where(lane >= s, jnp.maximum(cm, pltpu.roll(cm, s, 1)), cm)
    last = jnp.broadcast_to(cum[:, L - 1 :], (2 * CH, L))
    peak = jnp.broadcast_to(cm[:, L - 1 :], (2 * CH, L))
    weight = jnp.exp(a - peak)
    mm = last + peak
    rows[0], rows[1], rows[2], rows[3] = a, weight, last, mm
    colt[...] = jnp.transpose(jnp.concatenate([cm, cum, jnp.zeros((96, L), F32)], axis=0))

    ld_k.wait()
    ld_v.wait()

    def chunk_state(j, _):
        at = pl.ds(pl.multiple_of(j * L, L), L)
        for h in range(2):
            kt = jnp.transpose(k[at, h * DK : (h + 1) * DK].astype(F32))
            kw = kt * rows[1, pl.ds(2 * j + h, 1), :]
            dc[j, h, :, :DV] = jnp.dot(
                kw.astype(BF), v[at, h * DV : (h + 1) * DV], preferred_element_type=F32
            )
            dc[j, h, :, DV:] = jnp.broadcast_to(jnp.sum(kw, axis=1, keepdims=True), (DK, L))
        return 0

    lax.fori_loop(0, CH, chunk_state, 0)

    for h in range(2):
        tot = jnp.zeros((1, L), F32)
        logs = [None] * CH
        for j in reversed(range(CH)):
            row = 2 * j + h
            logs[j] = mm[row : row + 1] + tot
            tot = tot + last[row : row + 1]
        m = logs[0]
        for j in range(1, CH):
            m = jnp.maximum(m, logs[j])
        total = jnp.zeros((DK, DV + L), F32)
        for j in range(CH):
            total = total + jnp.exp(logs[j] - m)[:, 0:1] * dc[j, h]
        st1[h] = total[:, :DV].astype(BF)
        n_row = jnp.transpose(total[:, DV:])[0:1]
        ax1[h] = jnp.concatenate([n_row, tot, m, jnp.zeros((5, L), F32)], axis=0)

    s1 = [send(st1, st1r, {"sp_2": other}), send(ax1, ax1r, {"sp_2": other})]

    ld_q.wait()

    def within(j, _):
        at = pl.ds(pl.multiple_of(j * L, L), L)
        turned = pltpu.roll(colt[...], lax.rem(L - 2 * j, L), 1)
        for h in range(2):
            raw = lax.dot_general(
                q[at, h * DK : (h + 1) * DK], k[at, h * DK : (h + 1) * DK],
                (((1,), (1,)), ((), ())), preferred_element_type=F32,
            ) * SCALE
            logit = rows[0, pl.ds(2 * j + h, 1), :] - turned[:, h : h + 1]
            sc = raw * jnp.exp(jnp.where(causal, logit, NEG))
            nl[j, h, :, :DV] = jnp.dot(
                sc.astype(BF), v[at, h * DV : (h + 1) * DV], preferred_element_type=F32
            )
            nl[j, h, :, DV:] = jnp.broadcast_to(jnp.sum(sc, axis=1, keepdims=True), (L, L))
        return 0

    lax.fori_loop(0, 2, within, 0)

    cf = jnp.full((1, L), c, jnp.int32).astype(F32)
    arrived(s1)

    def aux(ref, *at):
        block = ref[at] if at else ref[...]
        return block[0:1], block[1:2], block[2:3]

    def pack(n, tot, m):
        return jnp.concatenate([n, tot, m, jnp.zeros((5, L), F32)], axis=0)

    n_o, t_o, m_o = aux(ax1, c)
    n_r, t_r, m_r = aux(ax1r, c)
    log_o = m_o + (1.0 - cf) * t_r
    log_r = m_r + cf * t_o
    m = jnp.maximum(log_o, log_r)
    w_o, w_r = jnp.exp(log_o - m), jnp.exp(log_r - m)
    st2[0] = (w_o[:, 0:1] * st1[c].astype(F32) + w_r[:, 0:1] * st1r[c].astype(F32)).astype(BF)
    ax2[0] = pack(w_o * n_o + w_r * n_r, t_o + t_r, m)
    s2 = []
    for n in (1, 2, 3):
        s2.append(send(st2.at[0], st2.at[n], {"sp_1": up(y, n)}))
        s2.append(send(ax2.at[0], ax2.at[n], {"sp_1": up(y, n)}))

    lax.fori_loop(2, 5, within, 0)

    def scan_of(st, ax, me, whole):
        parts = [aux(ax, n) for n in range(4)]
        mine = jnp.full((1, L), me, jnp.int32)
        below = [None] + [mine >= n for n in (1, 2, 3)]
        zero = jnp.zeros((1, L), F32)
        after = zero
        for n in (1, 2, 3):
            after = after + jnp.where(below[n], 0.0, parts[n][1])
        run, run_up = zero, zero
        log_in, log_all = [None] * 4, [parts[0][2] + after] + [None] * 3
        for n in (1, 2, 3):
            log_in[n] = jnp.where(below[n], parts[n][2] + run, NEG)
            log_all[n] = jnp.where(
                below[n], parts[n][2] + run + parts[0][1] + after, parts[n][2] + run_up
            )
            run = run + jnp.where(below[n], parts[n][1], 0.0)
            run_up = run_up + jnp.where(below[n], 0.0, parts[n][1])
        m_in = jnp.maximum(jnp.maximum(log_in[1], log_in[2]), log_in[3])
        w_in = [None] + [jnp.where(below[n], jnp.exp(log_in[n] - m_in), 0.0) for n in (1, 2, 3)]
        blocks = [st[n].astype(F32) for n in range(4)]
        c_in = sum(w_in[n][:, 0:1] * blocks[n] for n in (1, 2, 3))
        n_in = sum(w_in[n] * parts[n][0] for n in (1, 2, 3))
        inside = (c_in, n_in, run, m_in)
        if not whole:
            return inside, None
        m_all = jnp.maximum(
            jnp.maximum(log_all[0], log_all[1]), jnp.maximum(log_all[2], log_all[3])
        )
        w_all = [jnp.exp(t - m_all) for t in log_all]
        c_all = sum(w_all[n][:, 0:1] * blocks[n] for n in range(4))
        n_all = sum(w_all[n] * parts[n][0] for n in range(4))
        return inside, (c_all, n_all, run + run_up + parts[0][1], m_all)

    arrived(s2)
    y_in, y_all = scan_of(st2, ax2, y, True)
    st3[0] = y_all[0].astype(BF)
    ax3[0] = pack(*y_all[1:])
    s3 = []
    for n in (1, 2, 3):
        s3.append(send(st3.at[0], st3.at[n], {"sp_0": up(z, n)}))
        s3.append(send(ax3.at[0], ax3.at[n], {"sp_0": up(z, n)}))
    cpri[0, :, :DV] = y_in[0]

    lax.fori_loop(5, CH, within, 0)

    arrived(s3)
    z_in, _ = scan_of(st3, ax3, z, False)
    m = jnp.maximum(y_in[2] + z_in[3], y_in[3])
    w_z, w_y = jnp.exp(y_in[2] + z_in[3] - m), jnp.exp(y_in[3] - m)
    st4[...] = (w_z[:, 0:1] * z_in[0] + w_y[:, 0:1] * cpri[0, :, :DV]).astype(BF)
    ax4[...] = pack(w_z * z_in[1] + w_y * y_in[1], z_in[2] + y_in[2], m)
    s4 = [send(st4, st4r, {"sp_2": other}), send(ax4, ax4r, {"sp_2": other})]

    arrived(p1)
    p2 = []
    for ref in (wgv, wd):
        for src, dev in (
            (halves(ref, z, y3, 0, 16), {"sp_1": y1}),
            (halves(ref, z, y1, 16, 16), {"sp_1": y3}),
            (halves(ref, z3, y, 32, 16), {"sp_0": z1}),
            (halves(ref, z1, y, 48, 16), {"sp_0": z3}),
        ):
            p2.append(send(src, src, dev))

    arrived(s4)
    last_in = jnp.full((1, L), c, jnp.int32) == 1
    for h, st, ax in ((c, st4, ax4), (other, st4r, ax4r)):
        n_b, t_b, m_b = aux(ax)
        n_p, t_p, m_p = aux(ax1r, h)
        m_p = jnp.where(last_in, m_p, NEG)
        m_b = m_b + cf * t_p
        m = jnp.maximum(m_b, m_p)
        w_b, w_p = jnp.exp(m_b - m), jnp.where(last_in, jnp.exp(m_p - m), 0.0)
        cpri[h, :, :DV] = w_b[:, 0:1] * st[...].astype(F32) + w_p[:, 0:1] * st1r[h].astype(F32)
        n_row = w_b * n_b + w_p * n_p
        cpri[h, :, DV:] = jnp.transpose(jnp.broadcast_to(n_row, (L, L)))
        mpri[h] = m

    def carry(j, _):
        for h in range(2):
            state, m_old = cpri[h], mpri[h]
            cs[j, h] = state.astype(BF)
            row = pl.ds(2 * j + h, 1)
            rs_rows[row, :] = m_old
            decayed, fresh = rows[2, row, :] + m_old, rows[3, row, :]
            m_new = jnp.maximum(decayed, fresh)
            cpri[h] = (
                jnp.exp(decayed - m_new)[:, 0:1] * state
                + jnp.exp(fresh - m_new)[:, 0:1] * dc[j, h]
            )
            mpri[h] = m_new
        return 0

    lax.fori_loop(0, CH, carry, 0)

    ld_og.wait()

    def finish(j, _):
        at = pl.ds(pl.multiple_of(j * L, L), L)
        turned = pltpu.roll(colt[...], lax.rem(L - 2 * j, L), 1)
        for h in range(2):
            r = rs_rows[pl.ds(2 * j + h, 1), :][:, 0:1]
            cmc, cuc = turned[:, h : h + 1], turned[:, 16 + h : 17 + h]
            g = jnp.maximum(cmc, r)
            e1, e2 = jnp.exp(cmc - g), jnp.exp(r - g) * SCALE
            qc = jnp.dot(q[at, h * DK : (h + 1) * DK], cs[j, h], preferred_element_type=F32)
            both = e1 * nl[j, h] + e2 * qc
            inv = 1.0 / jnp.maximum(jnp.abs(both[:, DV:]), jnp.exp(-cuc - g))
            mo = both[:, :DV] * jnp.concatenate([inv, inv], axis=1)
            norm = lax.rsqrt(jnp.mean(mo * mo, axis=1, keepdims=True) + EPS)
            gate = jax.nn.sigmoid(og[at, h * DV : (h + 1) * DV].astype(F32))
            gated[at, h * DV : (h + 1) * DV] = (mo * norm * gain[h : h + 1, :] * gate).astype(BF)
        return 0

    a2a = []
    for n in (2, 1, 3, 0):
        b = up(tp, n)
        lax.fori_loop(2 * b, 2 * b + 2, finish, 0)
        block = pl.ds(pl.multiple_of(b * 256, 256), 256)
        if n:
            a2a.append(send(gated.at[block], orr.at[tp], {"tp": b}))
        else:
            orr[tp] = gated[block, :]
        if n == 1:
            arrived(w1)
            w2 = []
            for src, lo, dev in ((x3, 0, x1), (x1, 128, x3)):
                part = wo.at[src, pl.ds(c * 256 + lo, 128)]
                w2.append(send(part, part, {"tp": dev}))
            wpair = []
            for src in (x1, x3):
                part = wo.at[src, pl.ds(c * 256, 256)]
                wpair.append(send(part, part, {"sp_2": other}))

    def swap(ref, zz, yy, lo):
        part = ref.at[zz, yy, c, pl.ds(lo, 32)]
        return send(part, part, {"sp_2": other})

    arrived(p2)
    p3, pair = [], []
    for ref in (wgv, wd):
        row_a = ref.at[z, :, c, pl.ds(0, 32)]
        row_b = ref.at[:, y, c, pl.ds(32, 32)]
        p3 += [
            send(row_a, row_a, {"sp_0": z1}),
            send(row_a, row_a, {"sp_0": z3}),
            send(row_b, row_b, {"sp_1": y1}),
            send(row_b, row_b, {"sp_1": y3}),
        ]
        pair.append(send(row_a, row_a, {"sp_2": other}))
        pair.append(send(row_b, row_b, {"sp_2": other}))

    arrived(w2)
    part = wo.at[x2, pl.ds(c * 256, 256)]
    wpair.append(send(part, part, {"sp_2": other}))
    arrived(a2a)
    arrived(wpair)
    ld_res.wait()

    def project(n, ss):
        cols = pl.ds(pl.multiple_of(n * 256, 256), 256)
        acc = rsd[:, cols].astype(F32)
        for t in range(4):
            acc = acc + jnp.dot(orr[t], wo[t, :, cols], preferred_element_type=F32)
        low = acc.astype(BF)
        stream[:, cols] = low
        wide = low.astype(F32)
        sq = wide * wide
        return ss + sq[:, :L] + sq[:, L:]

    ss = lax.fori_loop(0, 8, project, jnp.zeros((256, L), F32))
    norm = lax.rsqrt(jnp.sum(ss, axis=1, keepdims=True) * (1.0 / D) + EPS)

    def normed(n, _):
        cols = pl.ds(pl.multiple_of(n * 256, 256), 256)
        rows_n = (stream[:, cols].astype(F32) * norm * fgain[:, cols]).astype(BF)
        gr[tp, pl.ds(16, 256), cols] = rows_n
        hs[:, cols] = rows_n[254:256].astype(F32)
        return 0

    lax.fori_loop(0, 8, normed, 0)

    hr[tp] = hs[...]
    halo = [send(hs, hr.at[tp], {"tp": up(tp, n)}) for n in (1, 2, 3)]
    s_next = [take("s") for _ in range(4)]
    r_next = take("r")

    def next_copy(t):
        return pltpu.make_async_remote_copy(
            src_ref=hs, dst_ref=hp, send_sem=ssem.at[s_next[t]], recv_sem=rsem.at[r_next],
            device_id={**at_place(place + 1), "tp": t}, device_id_type=MESH,
        )

    @pl.when(tp == 3)
    def _():
        for t in range(4):
            next_copy(t).start()

    own_rows = gr.at[tp, pl.ds(16, 256)]
    g1 = [send(own_rows, own_rows, {"tp": x1}), send(own_rows, own_rows, {"tp": x3})]

    arrived(p3)
    p4 = []
    for ref in (wgv, wd):
        for src, dev in (
            (ref.at[z3, :, c, pl.ds(0, 16)], {"sp_0": z1}),
            (ref.at[z1, :, c, pl.ds(16, 16)], {"sp_0": z3}),
            (ref.at[:, y3, c, pl.ds(32, 16)], {"sp_1": y1}),
            (ref.at[:, y1, c, pl.ds(48, 16)], {"sp_1": y3}),
        ):
            p4.append(send(src, src, dev))
        for src in (
            ref.at[z1, :, c, pl.ds(0, 32)],
            ref.at[z3, :, c, pl.ds(0, 32)],
            ref.at[:, y1, c, pl.ds(32, 32)],
            ref.at[:, y3, c, pl.ds(32, 32)],
        ):
            pair.append(send(src, src, {"sp_2": other}))
    z2, y2 = up(z, 2), up(y, 2)
    arrived(p4)
    for ref in (wgv, wd):
        for src in (ref.at[z2, :, c, pl.ds(0, 32)], ref.at[:, y2, c, pl.ds(32, 32)]):
            pair.append(send(src, src, {"sp_2": other}))
    arrived(halo)
    next_copy(0).wait_recv()
    arrived(pair)

    first = jnp.full((2, D), place, jnp.int32) == 0

    def feed(b, slot):
        from_here = hr[up(b, 3)]
        from_before = jnp.where(first, 0.0, hp[...])
        is_zero = jnp.full((2, D), b, jnp.int32) == 0
        two = jnp.where(is_zero, from_before, from_here)
        gr[b, pl.ds(0, 16), :] = jnp.concatenate([jnp.zeros((14, D), F32), two], axis=0).astype(BF)

        def up_tile(n, _):
            wide = pl.ds(pl.multiple_of(n * 256, 256), 256)
            cols = pl.ds(pl.multiple_of(n * L, L), L)
            w = wgv[:, :, :, :, wide].reshape(D, 256)
            gv = jnp.dot(gr[b], w, preferred_element_type=F32)

            def conv(u, tap):
                return (
                    tap[0:1, cols] * u[14:270] + tap[1:2, cols] * u[15:271] + tap[2:3, cols] * u[16:272]
                )

            cg, cv = conv(gv[:, :L], gtap), conv(gv[:, L:], vtap)
            hid[:, cols] = (cg / (1.0 + jnp.exp(-cg)) * cv).astype(BF)
            return 0

        lax.fori_loop(0, NT, up_tile, 0)

        def down_tile(n, _):
            cols = pl.ds(pl.multiple_of(n * 256, 256), 256)
            w = wd[n // 2, pl.ds(2 * lax.rem(n, 2), 2)].reshape(256, FFD)
            p = lax.dot_general(
                hid[...], w, (((1,), (1,)), ((), ())), preferred_element_type=F32
            )
            ps[slot, :, cols] = p.astype(BF)
            return 0

        lax.fori_loop(0, 8, down_tile, 0)

    feed(tp, 0)
    arrived(g1)
    g2 = []
    for src, lo, dev in ((x3, 16, x1), (x1, 144, x3)):
        part = gr.at[src, pl.ds(lo, 128)]
        g2.append(send(part, part, {"tp": dev}))
    back = []
    for n in (1, 3, 2):
        if n == 2:
            arrived(g2)
        feed(up(tp, n), n)
        back.append(send(ps.at[n], rr.at[n], {"tp": up(tp, n)}))
    arrived(back)

    def add(n, _):
        cols = pl.ds(pl.multiple_of(n * 256, 256), 256)
        s = ps[0, :, cols].astype(F32)
        for t in (1, 2, 3):
            s = s + rr[t, :, cols].astype(F32)
        out[:, cols] = (stream[:, cols].astype(F32) + s).astype(BF)
        return 0

    lax.fori_loop(0, 8, add, 0)

    for cp in open_sends:
        cp.wait_send()

    @pl.when(tp == 3)
    def _():
        for t in range(4):
            next_copy(t).wait_send()


def local(
    residual_entry_input, query_matrix_rows, key_matrix_rows, value_matrix_rows,
    output_gate_logits, input_gate_logits, forget_gate_logits, forget_decay_offset,
    head_norm_gain, cell_output_weight, feedforward_norm_gain, gate_up_weight,
    value_up_weight, gate_filter_taps, value_filter_taps, down_projection_weight,
):
    def chunks(gate):
        return gate.T.reshape(2, CH, L).transpose(1, 0, 2).reshape(2 * CH, L)

    hbm = pl.BlockSpec(memory_space=pl.ANY)
    vmem = pl.BlockSpec(memory_space=pltpu.VMEM)
    scratch = [
        pltpu.VMEM((1024, 256), BF), pltpu.VMEM((1024, 256), BF), pltpu.VMEM((1024, 512), BF),
        pltpu.VMEM((1024, 512), BF), pltpu.VMEM((256, D), BF),
        pltpu.VMEM((4, 4, 2, 64, 2 * FFD), BF), pltpu.VMEM((4, 4, 2, 64, FFD), BF),
        pltpu.VMEM((4, 512, D), BF),
        pltpu.VMEM((CH, 2, DK, DV + L), F32), pltpu.VMEM((CH, 2, L, DV + L), F32),
        pltpu.VMEM((L, L), F32), pltpu.VMEM((4, 2 * CH, L), F32),
        pltpu.VMEM((CH, 2, DK, DV + L), BF), pltpu.VMEM((2, DK, DV + L), F32),
        pltpu.VMEM((2, 1, L), F32), pltpu.VMEM((2 * CH, L), F32),
        pltpu.VMEM((2, DK, DV), BF), pltpu.VMEM((2, 8, L), F32),
        pltpu.VMEM((2, DK, DV), BF), pltpu.VMEM((2, 8, L), F32),
        pltpu.VMEM((4, DK, DV), BF), pltpu.VMEM((4, 8, L), F32),
        pltpu.VMEM((4, DK, DV), BF), pltpu.VMEM((4, 8, L), F32),
        pltpu.VMEM((DK, DV), BF), pltpu.VMEM((8, L), F32),
        pltpu.VMEM((DK, DV), BF), pltpu.VMEM((8, L), F32),
        pltpu.VMEM((1024, 512), BF), pltpu.VMEM((4, 256, 512), BF), pltpu.VMEM((256, D), BF),
        pltpu.VMEM((4, 272, D), BF), pltpu.VMEM((2, D), F32), pltpu.VMEM((4, 2, D), F32),
        pltpu.VMEM((2, D), F32), pltpu.VMEM((256, FFD), BF),
        pltpu.VMEM((4, 256, D), BF), pltpu.VMEM((4, 256, D), BF),
        pltpu.SemaphoreType.DMA((32,)), pltpu.SemaphoreType.DMA((100,)),
        pltpu.SemaphoreType.DMA((100,)),
    ]
    return pl.pallas_call(
        kernel,
        out_shape=jax.ShapeDtypeStruct((256, D), BF),
        in_specs=[hbm, hbm, hbm, hbm, hbm, vmem, vmem, vmem, vmem, hbm, vmem, hbm, hbm, hbm, vmem, vmem],
        out_specs=vmem,
        scratch_shapes=scratch,
        compiler_params=pltpu.CompilerParams(
            collective_id=0, has_side_effects=True, vmem_limit_bytes=67_043_328
        ),
    )(
        residual_entry_input, query_matrix_rows, key_matrix_rows, value_matrix_rows,
        output_gate_logits, chunks(input_gate_logits), chunks(forget_gate_logits),
        chunks(forget_decay_offset), head_norm_gain, cell_output_weight,
        feedforward_norm_gain.reshape(1, D), gate_up_weight, value_up_weight,
        down_projection_weight.T, gate_filter_taps, value_filter_taps,
    )


def solution(mesh):
    split = Mesh(mesh.devices.reshape(4, 4, 2, mesh.shape["tp"]), SP_TP)
    placed = (
        P(SP_TP, None), P(SP, "tp"), P(SP, "tp"), P(SP, "tp"), P(SP, "tp"), P(SP, "tp"),
        P(SP, "tp"), P(SP, "tp"), P("tp", None), P("tp", None), P(), P(SP, "tp"), P(SP, "tp"),
        P(None, "tp"), P(None, "tp"), P("tp", SP),
    )
    return jax.shard_map(
        local, mesh=split, in_specs=placed, out_specs=P(SP_TP, None), check_vma=False
    )
```

time: 421 us -> 161 us (0.38)
  waiting for transfers between devices: 163 us -> 0 us
  Pallas kernels: 0 us -> 156 us
  local copies, waits for them, and re-layouts: 105 us -> 2.3 us
  matrix products: 62.1 us -> 0 us
  blocking collectives: 48.7 us -> 0 us
  other arithmetic: 23.2 us -> 0 us
  between operations: 14.1 us -> 0.01 us
    pallas_call x0 -> x1, Pallas kernels: none -> 156 us  [local(): pl.pallas_call(kernel, out_shape=jax.ShapeDtypeStruct((256, D), BF), in_s...]
    all_gather x5 -> x0, waiting for transfers between devices: 115 us -> none  [the longest x1 56.7 us: side_by_side(): lax.all_gather(both, axis, axis=dim, tiled=True)]
    dynamic_update_slice x16 -> x0, local copies, waits for them, and re-layouts: 66.9 us -> none  [local(): lax.scan(local_step, initial, (blocks(queries_low), blocks(keys_low), blo...]
    dot_general x46 -> x0, matrix products: 62.1 us -> none  [the longest x1 24.1 us: local(): jnp.dot(hidden, whole_down, preferred_element_type=jnp.float32)]
    reduce_scatter x1 -> x0, waiting for transfers between devices: 46.4 us -> none  [local(): lax.psum_scatter(jnp.dot(hidden, whole_down, preferred_element_type=jnp.f...]
    all_gather x3 -> x0, blocking collectives: 33.1 us -> none  [gathered_once(): both, at, found = (lax.all_gather(jnp.concatenate(lines), axis), 0, {})]
    all_to_all x1 -> x0, blocking collectives: 15.5 us -> none  [local(): lax.all_to_all(gated_rows, 'tp', split_axis=0, concat_axis=1, tiled=True)]
    dynamic_slice x24 -> x0, local copies, waits for them, and re-layouts: 9.84 us -> none  [local(): lax.scan(local_step, initial, (blocks(queries_low), blocks(keys_low), blo...]
  transfers between devices with their start and end apart: 7 -> 0, of which waited for: 4 -> 0; matrix products, arithmetic and copies ran while one was open for 34% -> 0% of each run, Pallas kernels for 0% -> 0%
where the time goes in v1:
time: 161 us; the launch traced here: 158 us
  Pallas kernels  156 us (97%)
  local copies, waits for them, and re-layouts  2.3 us (1%)
    pallas_call x1, Pallas kernels, local(): pl.pallas_call(kernel, out_shape=jax.ShapeDtypeStruct((256, D), BF), in_s...  156 us

profile of v1, /device:TPU:0, one launch (start us, length us, event | category | flops | bytes accessed | tf_op | source)
XLA Modules:
  0.0 158.0 jit_solution(5086952537720451234)
XLA Ops:
  0.0 155.7 %shard_map.154 = bf16[256,2048]{1,0:T(8,128)(2,1)} custom-call(bf16[256,2048]{1,0:T(8,128)(2,1)} %res.1, bf16[1024,256]{1,0:T(8,128)(2,1)} %q_in.1, bf16[1024,256]{1,0:T(8,128)(2,1)} %k_in.1, bf16[1024,512]{1,0:T(8,128)(2,1)} %v_in.1, bf16[1024,512]{1,0:T(8,128)(2,1)} %og_in.1, f32[16,128]{1,0:T(8,128)} %bitcast.24, f32[16,128]{1,0:T(8,128)} %bitcast.25, ...), custom_call_target="tpu_custom_call" | custom-call | tf_op jit(solution)/shard_map/pallas_call | solution.py:561
  155.7 2.3 %copy.21 = bf16[256,2048]{1,0:T(8,128)(2,1)} copy(bf16[256,2048]{1,0:T(8,128)(2,1)} %shard_map.154) | data formatting | bytes 2097152

commit v2 on v1

--- a/solution.py
+++ b/solution.py
@@ -34,7 +34,7 @@
     out,
     q, k, v, og, rsd, wgv, wd, wo, dc, nl, colt, rows, cs, cpri, mpri, rs_rows,
     st1, ax1, st1r, ax1r, st2, ax2, st3, ax3, st4, ax4, st4r, ax4r,
-    gated, orr, stream, gr, hs, hr, hp, hid, ps, rr,
+    gated, al, orr, stream, gr, hs, hr, hp, gvs, hid, ps, rl, rr,
     lsem, ssem, rsem,
 ):
     z, y, c, tp = (lax.axis_index(a) for a in SP_TP)
@@ -77,6 +77,10 @@
         for cp in copies:
             cp.wait_recv()
 
+    def mark(name):
+        pass
+
+    mark('entry')
     ld_k = load(k_in, k)
     ld_v = load(v_in, v)
     ld_w = [load(dwn, wd.at[z, y, c])]
@@ -113,6 +117,7 @@
     def halves(ref, zz, yy, lo, n):
         return ref.at[zz, yy, c, pl.ds(lo, n)]
 
+    mark('barrier_done')
     for cp in ld_w:
         cp.wait()
     p1 = []
@@ -124,10 +129,12 @@
             send(mine_b, mine_b, {"sp_0": z1}),
             send(mine_b, mine_b, {"sp_0": z3}),
         ]
+    mark('w_issued')
     ld_wo.wait()
     wo_half = wo.at[tp, pl.ds(c * 256, 256)]
     w1 = [send(wo_half, wo_half, {"tp": x1}), send(wo_half, wo_half, {"tp": x3})]
 
+    mark('wo_issued')
     il = 15.0 * jnp.tanh(ig[...] / 15.0)
     xf = 15.0 * jnp.tanh(fg[...] / 15.0)
     fl = jnp.minimum(xf, 0.0) - log1p_of(jnp.exp(-jnp.abs(xf))) + off[...]
@@ -148,6 +155,7 @@
     rows[0], rows[1], rows[2], rows[3] = a, weight, last, mm
     colt[...] = jnp.transpose(jnp.concatenate([cm, cum, jnp.zeros((96, L), F32)], axis=0))
 
+    mark('gates')
     ld_k.wait()
     ld_v.wait()
 
@@ -164,6 +172,7 @@
 
     lax.fori_loop(0, CH, chunk_state, 0)
 
+    mark('chunkstates')
     for h in range(2):
         tot = jnp.zeros((1, L), F32)
         logs = [None] * CH
@@ -181,6 +190,7 @@
         n_row = jnp.transpose(total[:, DV:])[0:1]
         ax1[h] = jnp.concatenate([n_row, tot, m, jnp.zeros((5, L), F32)], axis=0)
 
+    mark('devstate')
     s1 = [send(st1, st1r, {"sp_2": other}), send(ax1, ax1r, {"sp_2": other})]
 
     ld_q.wait()
@@ -203,6 +213,7 @@
 
     lax.fori_loop(0, 2, within, 0)
 
+    mark('within2')
     cf = jnp.full((1, L), c, jnp.int32).astype(F32)
     arrived(s1)
 
@@ -213,6 +224,7 @@
     def pack(n, tot, m):
         return jnp.concatenate([n, tot, m, jnp.zeros((5, L), F32)], axis=0)
 
+    mark('s1_arr')
     n_o, t_o, m_o = aux(ax1, c)
     n_r, t_r, m_r = aux(ax1r, c)
     log_o = m_o + (1.0 - cf) * t_r
@@ -226,6 +238,7 @@
         s2.append(send(st2.at[0], st2.at[n], {"sp_1": up(y, n)}))
         s2.append(send(ax2.at[0], ax2.at[n], {"sp_1": up(y, n)}))
 
+    mark('s2_sent')
     lax.fori_loop(2, 5, within, 0)
 
     def scan_of(st, ax, me, whole):
@@ -261,7 +274,9 @@
         n_all = sum(w_all[n] * parts[n][0] for n in range(4))
         return inside, (c_all, n_all, run + run_up + parts[0][1], m_all)
 
+    mark('within5')
     arrived(s2)
+    mark('s2_arr')
     y_in, y_all = scan_of(st2, ax2, y, True)
     st3[0] = y_all[0].astype(BF)
     ax3[0] = pack(*y_all[1:])
@@ -271,16 +286,7 @@
         s3.append(send(ax3.at[0], ax3.at[n], {"sp_0": up(z, n)}))
     cpri[0, :, :DV] = y_in[0]
 
-    lax.fori_loop(5, CH, within, 0)
-
-    arrived(s3)
-    z_in, _ = scan_of(st3, ax3, z, False)
-    m = jnp.maximum(y_in[2] + z_in[3], y_in[3])
-    w_z, w_y = jnp.exp(y_in[2] + z_in[3] - m), jnp.exp(y_in[3] - m)
-    st4[...] = (w_z[:, 0:1] * z_in[0] + w_y[:, 0:1] * cpri[0, :, :DV]).astype(BF)
-    ax4[...] = pack(w_z * z_in[1] + w_y * y_in[1], z_in[2] + y_in[2], m)
-    s4 = [send(st4, st4r, {"sp_2": other}), send(ax4, ax4r, {"sp_2": other})]
-
+    mark('s3_sent')
     arrived(p1)
     p2 = []
     for ref in (wgv, wd):
@@ -291,8 +297,64 @@
             (halves(ref, z1, y, 48, 16), {"sp_0": z3}),
         ):
             p2.append(send(src, src, dev))
-
+    mark('p2_sent')
+    lax.fori_loop(5, CH, within, 0)
+
+    mark('within8')
+    arrived(s3)
+    mark('s3_arr')
+    z_in, _ = scan_of(st3, ax3, z, False)
+    m = jnp.maximum(y_in[2] + z_in[3], y_in[3])
+    w_z, w_y = jnp.exp(y_in[2] + z_in[3] - m), jnp.exp(y_in[3] - m)
+    st4[...] = (w_z[:, 0:1] * z_in[0] + w_y[:, 0:1] * cpri[0, :, :DV]).astype(BF)
+    ax4[...] = pack(w_z * z_in[1] + w_y * y_in[1], z_in[2] + y_in[2], m)
+    s4 = [send(st4, st4r, {"sp_2": other}), send(ax4, ax4r, {"sp_2": other})]
+
+    def across(ref):
+        row_a = ref.at[z, :, c, pl.ds(0, 32)]
+        row_b = ref.at[:, y, c, pl.ds(32, 32)]
+        return [
+            send(row_a, row_a, {"sp_0": z1}),
+            send(row_a, row_a, {"sp_0": z3}),
+            send(row_b, row_b, {"sp_1": y1}),
+            send(row_b, row_b, {"sp_1": y3}),
+        ], [send(row_a, row_a, {"sp_2": other}), send(row_b, row_b, {"sp_2": other})]
+
+    def across_two(ref):
+        far = [
+            send(src, src, dev)
+            for src, dev in (
+                (ref.at[z3, :, c, pl.ds(0, 16)], {"sp_0": z1}),
+                (ref.at[z1, :, c, pl.ds(16, 16)], {"sp_0": z3}),
+                (ref.at[:, y3, c, pl.ds(32, 16)], {"sp_1": y1}),
+                (ref.at[:, y1, c, pl.ds(48, 16)], {"sp_1": y3}),
+            )
+        ]
+        swap = [
+            send(src, src, {"sp_2": other})
+            for src in (
+                ref.at[z1, :, c, pl.ds(0, 32)],
+                ref.at[z3, :, c, pl.ds(0, 32)],
+                ref.at[:, y1, c, pl.ds(32, 32)],
+                ref.at[:, y3, c, pl.ds(32, 32)],
+            )
+        ]
+        return far, swap
+
+    def last_swap(ref):
+        z2, y2 = up(z, 2), up(y, 2)
+        return [
+            send(src, src, {"sp_2": other})
+            for src in (ref.at[z2, :, c, pl.ds(0, 32)], ref.at[:, y2, c, pl.ds(32, 32)])
+        ]
+
+    mark('s4_sent')
+    arrived(p2)
+    mark('p2_arr')
+    g_far1, g_pair = across(wgv)
+    mark('p3_sent')
     arrived(s4)
+    mark('s4_arr')
     last_in = jnp.full((1, L), c, jnp.int32) == 1
     for h, st, ax in ((c, st4, ax4), (other, st4r, ax4r)):
         n_b, t_b, m_b = aux(ax)
@@ -321,8 +383,10 @@
             mpri[h] = m_new
         return 0
 
+    mark('prior')
     lax.fori_loop(0, CH, carry, 0)
 
+    mark('carried')
     ld_og.wait()
 
     def finish(j, _):
@@ -347,44 +411,52 @@
         b = up(tp, n)
         lax.fori_loop(2 * b, 2 * b + 2, finish, 0)
         block = pl.ds(pl.multiple_of(b * 256, 256), 256)
-        if n:
+        half0 = pl.ds(pl.multiple_of(b * 256, 128), 128)
+        half1 = pl.ds(pl.multiple_of(b * 256 + 128, 128), 128)
+        if n == 2:
+            first_leg = [
+                send(gated.at[half0], al.at[0], {"tp": x1}),
+                send(gated.at[half1], al.at[1], {"tp": x3}),
+            ]
+        elif n:
             a2a.append(send(gated.at[block], orr.at[tp], {"tp": b}))
         else:
             orr[tp] = gated[block, :]
-        if n == 1:
-            arrived(w1)
-            w2 = []
-            for src, lo, dev in ((x3, 0, x1), (x1, 128, x3)):
-                part = wo.at[src, pl.ds(c * 256 + lo, 128)]
-                w2.append(send(part, part, {"tp": dev}))
-            wpair = []
-            for src in (x1, x3):
-                part = wo.at[src, pl.ds(c * 256, 256)]
-                wpair.append(send(part, part, {"sp_2": other}))
-
-    def swap(ref, zz, yy, lo):
-        part = ref.at[zz, yy, c, pl.ds(lo, 32)]
-        return send(part, part, {"sp_2": other})
-
-    arrived(p2)
-    p3, pair = [], []
-    for ref in (wgv, wd):
-        row_a = ref.at[z, :, c, pl.ds(0, 32)]
-        row_b = ref.at[:, y, c, pl.ds(32, 32)]
-        p3 += [
-            send(row_a, row_a, {"sp_0": z1}),
-            send(row_a, row_a, {"sp_0": z3}),
-            send(row_b, row_b, {"sp_1": y1}),
-            send(row_b, row_b, {"sp_1": y3}),
-        ]
-        pair.append(send(row_a, row_a, {"sp_2": other}))
-        pair.append(send(row_b, row_b, {"sp_2": other}))
-
+        if n == 3:
+            arrived(first_leg)
+            relayed = [
+                send(al.at[0], orr.at[x3, pl.ds(0, 128)], {"tp": x1}),
+                send(al.at[1], orr.at[x1, pl.ds(128, 128)], {"tp": x3}),
+            ]
+    mark('before_w1')
+    arrived(w1)
+    mark('w1_arr')
+    w2 = []
+    for src, lo, dev in ((x3, 0, x1), (x1, 128, x3)):
+        part = wo.at[src, pl.ds(c * 256 + lo, 128)]
+        w2.append(send(part, part, {"tp": dev}))
+    wpair = []
+    for src in (x1, x3):
+        part = wo.at[src, pl.ds(c * 256, 256)]
+        wpair.append(send(part, part, {"sp_2": other}))
+
+    mark('cell_done')
+    arrived(g_far1)
+    mark('gfar1_arr')
+    g_far2, more = across_two(wgv)
+    g_pair += more
+    d_far1, d_pair = across(wd)
+
+    mark('p3_sent')
     arrived(w2)
     part = wo.at[x2, pl.ds(c * 256, 256)]
     wpair.append(send(part, part, {"sp_2": other}))
+    mark('w2_arr')
+    arrived(relayed)
     arrived(a2a)
+    mark('a2a_arr')
     arrived(wpair)
+    mark('wpair_arr')
     ld_res.wait()
 
     def project(n, ss):
@@ -399,6 +471,7 @@
         return ss + sq[:, :L] + sq[:, L:]
 
     ss = lax.fori_loop(0, 8, project, jnp.zeros((256, L), F32))
+    mark('projected')
     norm = lax.rsqrt(jnp.sum(ss, axis=1, keepdims=True) * (1.0 / D) + EPS)
 
     def normed(n, _):
@@ -410,6 +483,7 @@
 
     lax.fori_loop(0, 8, normed, 0)
 
+    mark('normed')
     hr[tp] = hs[...]
     halo = [send(hs, hr.at[tp], {"tp": up(tp, n)}) for n in (1, 2, 3)]
     s_next = [take("s") for _ in range(4)]
@@ -429,96 +503,166 @@
     own_rows = gr.at[tp, pl.ds(16, 256)]
     g1 = [send(own_rows, own_rows, {"tp": x1}), send(own_rows, own_rows, {"tp": x3})]
 
-    arrived(p3)
-    p4 = []
-    for ref in (wgv, wd):
-        for src, dev in (
-            (ref.at[z3, :, c, pl.ds(0, 16)], {"sp_0": z1}),
-            (ref.at[z1, :, c, pl.ds(16, 16)], {"sp_0": z3}),
-            (ref.at[:, y3, c, pl.ds(32, 16)], {"sp_1": y1}),
-            (ref.at[:, y1, c, pl.ds(48, 16)], {"sp_1": y3}),
-        ):
-            p4.append(send(src, src, dev))
-        for src in (
-            ref.at[z1, :, c, pl.ds(0, 32)],
-            ref.at[z3, :, c, pl.ds(0, 32)],
-            ref.at[:, y1, c, pl.ds(32, 32)],
-            ref.at[:, y3, c, pl.ds(32, 32)],
-        ):
-            pair.append(send(src, src, {"sp_2": other}))
-    z2, y2 = up(z, 2), up(y, 2)
-    arrived(p4)
-    for ref in (wgv, wd):
-        for src in (ref.at[z2, :, c, pl.ds(0, 32)], ref.at[:, y2, c, pl.ds(32, 32)]):
-            pair.append(send(src, src, {"sp_2": other}))
+    mark('g1_sent')
+    arrived(g_far2)
+    mark('gfar2_arr')
+    g_pair += last_swap(wgv)
+    arrived(d_far1)
+    mark('dfar1_arr')
+    d_far2, more = across_two(wd)
+    d_pair += more
     arrived(halo)
     next_copy(0).wait_recv()
-    arrived(pair)
+    mark('halo_arr')
+    arrived(g_pair)
+    mark('gpair_arr')
 
     first = jnp.full((2, D), place, jnp.int32) == 0
 
-    def feed(b, slot):
+    def copy_of(src, dst, dev):
+        cp = pltpu.make_async_remote_copy(
+            src_ref=src, dst_ref=dst, send_sem=ssem.at[take("s")], recv_sem=rsem.at[take("r")],
+            device_id=dev, device_id_type=MESH,
+        )
+        open_sends.append(cp)
+        return cp
+
+    lo, hi = pl.ds(0, 128), pl.ds(128, 128)
+    part_a, part_b = gr.at[x3, pl.ds(16, 128)], gr.at[x1, pl.ds(144, 128)]
+    g2 = [copy_of(part_a, part_a, {"tp": x1}), copy_of(part_b, part_b, {"tp": x3})]
+    far = [
+        copy_of(ps.at[2, lo], rl.at[0], {"tp": x1}),
+        copy_of(ps.at[2, hi], rl.at[1], {"tp": x3}),
+    ]
+    direct = [
+        copy_of(ps.at[1, hi], rr.at[0, hi], {"tp": x1}),
+        copy_of(ps.at[3, lo], rr.at[1, lo], {"tp": x3}),
+    ]
+    summed = [
+        copy_of(ps.at[1, lo], rr.at[0, lo], {"tp": x1}),
+        copy_of(ps.at[3, hi], rr.at[1, hi], {"tp": x3}),
+    ]
+    d_near = list(d_pair)
+    z2, y2 = up(z, 2), up(y, 2)
+    d_last = [
+        copy_of(src, src, {"sp_2": other})
+        for src in (wd.at[z2, :, c, pl.ds(0, 32)], wd.at[:, y2, c, pl.ds(32, 32)])
+    ]
+
+    def feed(i, _):
+        slot = i ^ (i >> 1)
+        b = up(tp, slot)
+
+        @pl.when(i == 1)
+        def _():
+            mark('feed0')
+            arrived(g1)
+            mark('g1_arr')
+            for cp in g2:
+                cp.start()
+
+        @pl.when(i == 3)
+        def _():
+            mark('feed2')
+            arrived(g2)
+            mark('g2_arr')
+
         from_here = hr[up(b, 3)]
         from_before = jnp.where(first, 0.0, hp[...])
         is_zero = jnp.full((2, D), b, jnp.int32) == 0
         two = jnp.where(is_zero, from_before, from_here)
         gr[b, pl.ds(0, 16), :] = jnp.concatenate([jnp.zeros((14, D), F32), two], axis=0).astype(BF)
 
-        def up_tile(n, _):
-            wide = pl.ds(pl.multiple_of(n * 256, 256), 256)
-            cols = pl.ds(pl.multiple_of(n * L, L), L)
-            w = wgv[:, :, :, :, wide].reshape(D, 256)
-            gv = jnp.dot(gr[b], w, preferred_element_type=F32)
-
-            def conv(u, tap):
+        def product(n):
+            w = wgv[:, :, :, :, n * 256 : n * 256 + 256].reshape(D, 256)
+            gvs[n % 2] = jnp.dot(gr[b], w, preferred_element_type=F32)
+
+        def gate_of(n):
+            cols = slice(n * L, n * L + L)
+
+            def conv(lanes, tap):
                 return (
-                    tap[0:1, cols] * u[14:270] + tap[1:2, cols] * u[15:271] + tap[2:3, cols] * u[16:272]
+                    tap[0:1, cols] * gvs[n % 2, 14:270, lanes]
+                    + tap[1:2, cols] * gvs[n % 2, 15:271, lanes]
+                    + tap[2:3, cols] * gvs[n % 2, 16:272, lanes]
                 )
 
-            cg, cv = conv(gv[:, :L], gtap), conv(gv[:, L:], vtap)
+            cg, cv = conv(slice(0, L), gtap), conv(slice(L, 256), vtap)
             hid[:, cols] = (cg / (1.0 + jnp.exp(-cg)) * cv).astype(BF)
-            return 0
-
-        lax.fori_loop(0, NT, up_tile, 0)
-
-        def down_tile(n, _):
-            cols = pl.ds(pl.multiple_of(n * 256, 256), 256)
-            w = wd[n // 2, pl.ds(2 * lax.rem(n, 2), 2)].reshape(256, FFD)
+
+        product(0)
+        for n in range(1, NT):
+            product(n)
+            gate_of(n - 1)
+        gate_of(NT - 1)
+        mark('up_done')
+
+        @pl.when(i == 0)
+        def _():
+            arrived(d_far2)
+            mark('dfar2_arr')
+            for cp in d_last:
+                cp.start()
+            arrived(d_near)
+            arrived(d_last)
+            mark('dpair_arr')
+
+        for n in range(8):
+            w = wd[n // 2, 2 * (n % 2) : 2 * (n % 2) + 2].reshape(256, FFD)
             p = lax.dot_general(
                 hid[...], w, (((1,), (1,)), ((), ())), preferred_element_type=F32
             )
-            ps[slot, :, cols] = p.astype(BF)
+            ps[slot, :, n * 256 : n * 256 + 256] = p.astype(BF)
+        mark('down_done')
+
+        @pl.when(i == 1)
+        def _():
+            direct[0].start()
+
+        @pl.when(i == 2)
+        def _():
+            direct[1].start()
+
+        @pl.when(i == 3)
+        def _():
+            for cp in far:
+                cp.start()
+
+        return 0
+
+    lax.fori_loop(0, 4, feed, 0)
+    mark('fed')
+    for n, (cp, half) in enumerate(zip(far, (lo, hi))):
+        cp.wait_recv()
+        mark('far_arr')
+
+        def relay(m, _):
+            cols = pl.ds(pl.multiple_of(m * 256, 256), 256)
+            ps[2 * n + 1, half, cols] = (
+                ps[2 * n + 1, half, cols].astype(F32) + rl[n, :, cols].astype(F32)
+            ).astype(BF)
             return 0
 
-        lax.fori_loop(0, 8, down_tile, 0)
-
-    feed(tp, 0)
-    arrived(g1)
-    g2 = []
-    for src, lo, dev in ((x3, 16, x1), (x1, 144, x3)):
-        part = gr.at[src, pl.ds(lo, 128)]
-        g2.append(send(part, part, {"tp": dev}))
-    back = []
-    for n in (1, 3, 2):
-        if n == 2:
-            arrived(g2)
-        feed(up(tp, n), n)
-        back.append(send(ps.at[n], rr.at[n], {"tp": up(tp, n)}))
-    arrived(back)
+        lax.fori_loop(0, 8, relay, 0)
+        summed[n].start()
+    arrived(direct)
+    mark('direct_arr')
+    arrived(summed)
+    mark('back_arr')
 
     def add(n, _):
         cols = pl.ds(pl.multiple_of(n * 256, 256), 256)
-        s = ps[0, :, cols].astype(F32)
-        for t in (1, 2, 3):
-            s = s + rr[t, :, cols].astype(F32)
+        s = ps[0, :, cols].astype(F32) + rr[0, :, cols].astype(F32) + rr[1, :, cols].astype(F32)
         out[:, cols] = (stream[:, cols].astype(F32) + s).astype(BF)
         return 0
 
     lax.fori_loop(0, 8, add, 0)
 
+    mark('added')
     for cp in open_sends:
         cp.wait_send()
 
+    mark('sends_done')
     @pl.when(tp == 3)
     def _():
         for t in range(4):
@@ -551,10 +695,11 @@
         pltpu.VMEM((4, DK, DV), BF), pltpu.VMEM((4, 8, L), F32),
         pltpu.VMEM((DK, DV), BF), pltpu.VMEM((8, L), F32),
         pltpu.VMEM((DK, DV), BF), pltpu.VMEM((8, L), F32),
-        pltpu.VMEM((1024, 512), BF), pltpu.VMEM((4, 256, 512), BF), pltpu.VMEM((256, D), BF),
+        pltpu.VMEM((1024, 512), BF), pltpu.VMEM((2, 128, 512), BF), pltpu.VMEM((4, 256, 512), BF),
+        pltpu.VMEM((256, D), BF),
         pltpu.VMEM((4, 272, D), BF), pltpu.VMEM((2, D), F32), pltpu.VMEM((4, 2, D), F32),
-        pltpu.VMEM((2, D), F32), pltpu.VMEM((256, FFD), BF),
-        pltpu.VMEM((4, 256, D), BF), pltpu.VMEM((4, 256, D), BF),
+        pltpu.VMEM((2, D), F32), pltpu.VMEM((2, 272, 256), F32), pltpu.VMEM((256, FFD), BF),
+        pltpu.VMEM((4, 256, D), BF), pltpu.VMEM((2, 128, D), BF), pltpu.VMEM((2, 256, D), BF),
         pltpu.SemaphoreType.DMA((32,)), pltpu.SemaphoreType.DMA((100,)),
         pltpu.SemaphoreType.DMA((100,)),
     ]

time: 161 us -> 142 us (0.88); the launches traced: 158 us -> 141 us
  Pallas kernels: 156 us -> 139 us
    pallas_call x1, Pallas kernels: 156 us -> 139 us  [local(): pl.pallas_call(kernel, out_shape=jax.ShapeDtypeStruct((256, D), BF), in_s...]
where the time goes in v2:
time: 142 us; the launch traced here: 141 us
  Pallas kernels  139 us (98%)
  local copies, waits for them, and re-layouts  2.3 us (2%)
    pallas_call x1, Pallas kernels, local(): pl.pallas_call(kernel, out_shape=jax.ShapeDtypeStruct((256, D), BF), in_s...  139 us

profile of v2, /device:TPU:0, one launch (start us, length us, event | category | flops | bytes accessed | tf_op | source)
XLA Modules:
  0.0 141.3 jit_solution(1719649710718743877)
XLA Ops:
  0.0 139.0 %shard_map.154 = bf16[256,2048]{1,0:T(8,128)(2,1)} custom-call(bf16[256,2048]{1,0:T(8,128)(2,1)} %res.1, bf16[1024,256]{1,0:T(8,128)(2,1)} %q_in.1, bf16[1024,256]{1,0:T(8,128)(2,1)} %k_in.1, bf16[1024,512]{1,0:T(8,128)(2,1)} %v_in.1, bf16[1024,512]{1,0:T(8,128)(2,1)} %og_in.1, f32[16,128]{1,0:T(8,128)} %bitcast.24, f32[16,128]{1,0:T(8,128)} %bitcast.25, ...), custom_call_target="tpu_custom_call" | custom-call | tf_op jit(solution)/shard_map/pallas_call | solution.py:706
  139.0 2.3 %copy.21 = bf16[256,2048]{1,0:T(8,128)(2,1)} copy(bf16[256,2048]{1,0:T(8,128)(2,1)} %shard_map.154) | data formatting | bytes 2097152

commit v3 on v2

--- a/solution.py
+++ b/solution.py
@@ -131,8 +131,89 @@
         ]
     mark('w_issued')
     ld_wo.wait()
-    wo_half = wo.at[tp, pl.ds(c * 256, 256)]
-    w1 = [send(wo_half, wo_half, {"tp": x1}), send(wo_half, wo_half, {"tp": x3})]
+    y2, z2 = up(y, 2), up(z, 2)
+
+    def wo_pieces(t, far):
+        return wo.at[t, c, 0, y2 if far else y], wo.at[t, c, 1, z2 if far else z]
+
+    xo1a, xo1b = (
+        [send(piece, piece, {"tp": dev}) for piece in wo_pieces(tp, n) for dev in (x1, x3)]
+        for n in (False, True)
+    )
+
+    def wo_swap(piece):
+        return send(piece, piece, {"sp_2": other})
+
+    def wo_onward(far):
+        py, pz = wo_pieces(x3, far)[0], wo_pieces(x1, far)[1]
+        return [send(py, py, {"tp": x1}), send(pz, pz, {"tp": x3})]
+
+    def wo_spread(t):
+        py, pz = wo_pieces(t, False)
+        near = [
+            send(py, py, {"sp_1": y1}), send(py, py, {"sp_1": y3}),
+            send(pz, pz, {"sp_0": z1}), send(pz, pz, {"sp_0": z3}),
+        ]
+        return near, [wo_swap(py), wo_swap(pz)]
+
+    def wo_near_swaps(t):
+        return [
+            wo_swap(piece)
+            for piece in (
+                wo.at[t, c, 0, y1], wo.at[t, c, 0, y3], wo.at[t, c, 1, z1], wo.at[t, c, 1, z3]
+            )
+        ]
+
+    def slab(ref, n):
+        piece_a, piece_b = halves(ref, z, up(y, n), 0, 32), halves(ref, up(z, n), y, 32, 32)
+        return [
+            send(piece_a, piece_a, {"sp_0": z1}),
+            send(piece_a, piece_a, {"sp_0": z3}),
+            send(piece_b, piece_b, {"sp_1": y1}),
+            send(piece_b, piece_b, {"sp_1": y3}),
+        ]
+
+    def row_swap(ref):
+        row_a = ref.at[z, :, c, pl.ds(0, 32)]
+        row_b = ref.at[:, y, c, pl.ds(32, 32)]
+        return [send(row_a, row_a, {"sp_2": other}), send(row_b, row_b, {"sp_2": other})]
+
+    def across(ref):
+        row_a = ref.at[z, :, c, pl.ds(0, 32)]
+        row_b = ref.at[:, y, c, pl.ds(32, 32)]
+        return [
+            send(row_a, row_a, {"sp_0": z1}),
+            send(row_a, row_a, {"sp_0": z3}),
+            send(row_b, row_b, {"sp_1": y1}),
+            send(row_b, row_b, {"sp_1": y3}),
+        ]
+
+    def across_two(ref):
+        far = [
+            send(src, src, dev)
+            for src, dev in (
+                (ref.at[z3, :, c, pl.ds(0, 16)], {"sp_0": z1}),
+                (ref.at[z1, :, c, pl.ds(16, 16)], {"sp_0": z3}),
+                (ref.at[:, y3, c, pl.ds(32, 16)], {"sp_1": y1}),
+                (ref.at[:, y1, c, pl.ds(48, 16)], {"sp_1": y3}),
+            )
+        ]
+        swap = [
+            send(src, src, {"sp_2": other})
+            for src in (
+                ref.at[z1, :, c, pl.ds(0, 32)],
+                ref.at[z3, :, c, pl.ds(0, 32)],
+                ref.at[:, y1, c, pl.ds(32, 32)],
+                ref.at[:, y3, c, pl.ds(32, 32)],
+            )
+        ]
+        return far, swap
+
+    def last_swap(ref):
+        return [
+            send(src, src, {"sp_2": other})
+            for src in (ref.at[z2, :, c, pl.ds(0, 32)], ref.at[:, y2, c, pl.ds(32, 32)])
+        ]
 
     mark('wo_issued')
     il = 15.0 * jnp.tanh(ig[...] / 15.0)
@@ -287,6 +368,22 @@
     cpri[0, :, :DV] = y_in[0]
 
     mark('s3_sent')
+    arrived(xo1a)
+    xo2a = wo_onward(False)
+    near_a, wpair = wo_spread(x1)
+    near_b, more = wo_spread(x3)
+    wpair += more
+    mark('xo1_arr')
+    mark('p2_sent')
+    lax.fori_loop(5, CH, within, 0)
+
+    mark('within8')
+    arrived(xo1b)
+    xo2b = wo_onward(True)
+    arrived(xo2a)
+    mark('xo2_arr')
+    near_c, more = wo_spread(x2)
+    wpair += more
     arrived(p1)
     p2 = []
     for ref in (wgv, wd):
@@ -297,10 +394,7 @@
             (halves(ref, z1, y, 48, 16), {"sp_0": z3}),
         ):
             p2.append(send(src, src, dev))
-    mark('p2_sent')
-    lax.fori_loop(5, CH, within, 0)
-
-    mark('within8')
+    g_far1 = slab(wgv, 0) + slab(wgv, 1) + slab(wgv, 3)
     arrived(s3)
     mark('s3_arr')
     z_in, _ = scan_of(st3, ax3, z, False)
@@ -310,49 +404,7 @@
     ax4[...] = pack(w_z * z_in[1] + w_y * y_in[1], z_in[2] + y_in[2], m)
     s4 = [send(st4, st4r, {"sp_2": other}), send(ax4, ax4r, {"sp_2": other})]
 
-    def across(ref):
-        row_a = ref.at[z, :, c, pl.ds(0, 32)]
-        row_b = ref.at[:, y, c, pl.ds(32, 32)]
-        return [
-            send(row_a, row_a, {"sp_0": z1}),
-            send(row_a, row_a, {"sp_0": z3}),
-            send(row_b, row_b, {"sp_1": y1}),
-            send(row_b, row_b, {"sp_1": y3}),
-        ], [send(row_a, row_a, {"sp_2": other}), send(row_b, row_b, {"sp_2": other})]
-
-    def across_two(ref):
-        far = [
-            send(src, src, dev)
-            for src, dev in (
-                (ref.at[z3, :, c, pl.ds(0, 16)], {"sp_0": z1}),
-                (ref.at[z1, :, c, pl.ds(16, 16)], {"sp_0": z3}),
-                (ref.at[:, y3, c, pl.ds(32, 16)], {"sp_1": y1}),
-                (ref.at[:, y1, c, pl.ds(48, 16)], {"sp_1": y3}),
-            )
-        ]
-        swap = [
-            send(src, src, {"sp_2": other})
-            for src in (
-                ref.at[z1, :, c, pl.ds(0, 32)],
-                ref.at[z3, :, c, pl.ds(0, 32)],
-                ref.at[:, y1, c, pl.ds(32, 32)],
-                ref.at[:, y3, c, pl.ds(32, 32)],
-            )
-        ]
-        return far, swap
-
-    def last_swap(ref):
-        z2, y2 = up(z, 2), up(y, 2)
-        return [
-            send(src, src, {"sp_2": other})
-            for src in (ref.at[z2, :, c, pl.ds(0, 32)], ref.at[:, y2, c, pl.ds(32, 32)])
-        ]
-
     mark('s4_sent')
-    arrived(p2)
-    mark('p2_arr')
-    g_far1, g_pair = across(wgv)
-    mark('p3_sent')
     arrived(s4)
     mark('s4_arr')
     last_in = jnp.full((1, L), c, jnp.int32) == 1
@@ -422,35 +474,32 @@
             a2a.append(send(gated.at[block], orr.at[tp], {"tp": b}))
         else:
             orr[tp] = gated[block, :]
+        if n == 1:
+            mark('cell_two')
+            arrived(near_a)
+            arrived(near_b)
+            mark('near_ab')
+            wpair += wo_near_swaps(x1) + wo_near_swaps(x3)
+            for t in (x1, x3):
+                wpair += [wo_swap(piece) for piece in wo_pieces(t, True)]
         if n == 3:
+            mark('cell_three')
             arrived(first_leg)
+            mark('leg_arr')
             relayed = [
                 send(al.at[0], orr.at[x3, pl.ds(0, 128)], {"tp": x1}),
                 send(al.at[1], orr.at[x1, pl.ds(128, 128)], {"tp": x3}),
             ]
-    mark('before_w1')
-    arrived(w1)
-    mark('w1_arr')
-    w2 = []
-    for src, lo, dev in ((x3, 0, x1), (x1, 128, x3)):
-        part = wo.at[src, pl.ds(c * 256 + lo, 128)]
-        w2.append(send(part, part, {"tp": dev}))
-    wpair = []
-    for src in (x1, x3):
-        part = wo.at[src, pl.ds(c * 256, 256)]
-        wpair.append(send(part, part, {"sp_2": other}))
-
     mark('cell_done')
-    arrived(g_far1)
-    mark('gfar1_arr')
-    g_far2, more = across_two(wgv)
-    g_pair += more
-    d_far1, d_pair = across(wd)
-
-    mark('p3_sent')
-    arrived(w2)
-    part = wo.at[x2, pl.ds(c * 256, 256)]
-    wpair.append(send(part, part, {"sp_2": other}))
+    arrived(near_c)
+    mark('near_c')
+    arrived(xo2b)
+    wpair += wo_near_swaps(x2) + [wo_swap(piece) for piece in wo_pieces(x2, True)]
+    arrived(p2)
+    mark('p2_arr')
+    g_far1 += slab(wgv, 2)
+    g_pair = row_swap(wgv)
+
     mark('w2_arr')
     arrived(relayed)
     arrived(a2a)
@@ -463,7 +512,7 @@
         cols = pl.ds(pl.multiple_of(n * 256, 256), 256)
         acc = rsd[:, cols].astype(F32)
         for t in range(4):
-            acc = acc + jnp.dot(orr[t], wo[t, :, cols], preferred_element_type=F32)
+            acc = acc + jnp.dot(orr[t], wo[t, :, :, :, :, cols].reshape(512, 256), preferred_element_type=F32)
         low = acc.astype(BF)
         stream[:, cols] = low
         wide = low.astype(F32)
@@ -477,33 +526,52 @@
     def normed(n, _):
         cols = pl.ds(pl.multiple_of(n * 256, 256), 256)
         rows_n = (stream[:, cols].astype(F32) * norm * fgain[:, cols]).astype(BF)
-        gr[tp, pl.ds(16, 256), cols] = rows_n
-        hs[:, cols] = rows_n[254:256].astype(F32)
+        gr[2 * tp, pl.ds(16, 128), cols] = rows_n[:128]
+        gr[2 * tp + 1, pl.ds(16, 128), cols] = rows_n[128:]
+        hs[0, :, cols] = rows_n[254:256].astype(F32)
+        hs[1, :, cols] = rows_n[126:128].astype(F32)
         return 0
 
     lax.fori_loop(0, 8, normed, 0)
 
     mark('normed')
     hr[tp] = hs[...]
-    halo = [send(hs, hr.at[tp], {"tp": up(tp, n)}) for n in (1, 2, 3)]
     s_next = [take("s") for _ in range(4)]
     r_next = take("r")
 
     def next_copy(t):
         return pltpu.make_async_remote_copy(
-            src_ref=hs, dst_ref=hp, send_sem=ssem.at[s_next[t]], recv_sem=rsem.at[r_next],
+            src_ref=hs.at[0], dst_ref=hp, send_sem=ssem.at[s_next[t]], recv_sem=rsem.at[r_next],
             device_id={**at_place(place + 1), "tp": t}, device_id_type=MESH,
         )
 
+    def half_rows(b, h):
+        return gr.at[2 * b + h, pl.ds(16, 128)]
+
+    own_lo, own_hi = half_rows(tp, 0), half_rows(tp, 1)
+    g1a = [send(own_lo, own_lo, {"tp": x1}), send(own_hi, own_hi, {"tp": x3})]
+    halo = [send(hs, hr.at[tp], {"tp": up(tp, n)}) for n in (1, 2, 3)]
     @pl.when(tp == 3)
     def _():
         for t in range(4):
             next_copy(t).start()
 
-    own_rows = gr.at[tp, pl.ds(16, 256)]
-    g1 = [send(own_rows, own_rows, {"tp": x1}), send(own_rows, own_rows, {"tp": x3})]
+    g1b = [send(own_hi, own_hi, {"tp": x1}), send(own_lo, own_lo, {"tp": x3})]
 
     mark('g1_sent')
+    arrived(g_far1)
+    mark('gfar1_arr')
+    g_far2, more = across_two(wgv)
+    g_pair += more
+    d_far1 = across(wd)
+    d_pair = row_swap(wd)
+    arrived(halo)
+    next_copy(0).wait_recv()
+    mark('halo_arr')
+    arrived(g1a)
+    mark('g1a_arr')
+    part_a, part_b = half_rows(x3, 0), half_rows(x1, 1)
+    g2 = [send(part_a, part_a, {"tp": x1}), send(part_b, part_b, {"tp": x3})]
     arrived(g_far2)
     mark('gfar2_arr')
     g_pair += last_swap(wgv)
@@ -511,9 +579,6 @@
     mark('dfar1_arr')
     d_far2, more = across_two(wd)
     d_pair += more
-    arrived(halo)
-    next_copy(0).wait_recv()
-    mark('halo_arr')
     arrived(g_pair)
     mark('gpair_arr')
 
@@ -528,109 +593,117 @@
         return cp
 
     lo, hi = pl.ds(0, 128), pl.ds(128, 128)
-    part_a, part_b = gr.at[x3, pl.ds(16, 128)], gr.at[x1, pl.ds(144, 128)]
-    g2 = [copy_of(part_a, part_a, {"tp": x1}), copy_of(part_b, part_b, {"tp": x3})]
+    direct = [
+        copy_of(ps.at[0, lo], rr.at[0, hi], {"tp": x1}),
+        copy_of(ps.at[0, hi], rr.at[1, lo], {"tp": x3}),
+    ]
     far = [
         copy_of(ps.at[2, lo], rl.at[0], {"tp": x1}),
         copy_of(ps.at[2, hi], rl.at[1], {"tp": x3}),
     ]
-    direct = [
-        copy_of(ps.at[1, hi], rr.at[0, hi], {"tp": x1}),
-        copy_of(ps.at[3, lo], rr.at[1, lo], {"tp": x3}),
-    ]
     summed = [
         copy_of(ps.at[1, lo], rr.at[0, lo], {"tp": x1}),
-        copy_of(ps.at[3, hi], rr.at[1, hi], {"tp": x3}),
+        copy_of(ps.at[1, hi], rr.at[1, hi], {"tp": x3}),
     ]
-    d_near = list(d_pair)
-    z2, y2 = up(z, 2), up(y, 2)
-    d_last = [
-        copy_of(src, src, {"sp_2": other})
-        for src in (wd.at[z2, :, c, pl.ds(0, 32)], wd.at[:, y2, c, pl.ds(32, 32)])
-    ]
-
-    def feed(i, _):
-        slot = i ^ (i >> 1)
-        b = up(tp, slot)
-
-        @pl.when(i == 1)
-        def _():
-            mark('feed0')
-            arrived(g1)
-            mark('g1_arr')
-            for cp in g2:
-                cp.start()
-
-        @pl.when(i == 3)
-        def _():
-            mark('feed2')
-            arrived(g2)
-            mark('g2_arr')
-
-        from_here = hr[up(b, 3)]
-        from_before = jnp.where(first, 0.0, hp[...])
-        is_zero = jnp.full((2, D), b, jnp.int32) == 0
-        two = jnp.where(is_zero, from_before, from_here)
-        gr[b, pl.ds(0, 16), :] = jnp.concatenate([jnp.zeros((14, D), F32), two], axis=0).astype(BF)
+
+    def rows_of(i):
+        pair = i // 2
+        h0 = (1 - pair) * (1 - i)
+        b0 = up(tp, 1 - pair + pair * (6 - 2 * i))
+        b1 = up(tp, 3 * (1 - pair) + pair * (6 - 2 * i))
+        return (b0, h0), (b1, 1 - h0)
+
+    def widen(i):
+        spots = rows_of(i)
+        for b, h in spots:
+            from_last = jnp.where(
+                jnp.full((2, D), b, jnp.int32) == 0,
+                jnp.where(first, 0.0, hp[...]),
+                hr[up(b, 3), 0],
+            )
+            two = jnp.where(jnp.full((2, D), h, jnp.int32) == 1, hr[b, 1], from_last)
+            gr[2 * b + h, pl.ds(0, 16), :] = jnp.concatenate(
+                [jnp.zeros((14, D), F32), two], axis=0
+            ).astype(BF)
+        e0, e1 = (2 * b + h for b, h in spots)
 
         def product(n):
             w = wgv[:, :, :, :, n * 256 : n * 256 + 256].reshape(D, 256)
-            gvs[n % 2] = jnp.dot(gr[b], w, preferred_element_type=F32)
+            both = jnp.concatenate([gr[e0], gr[e1]], axis=0)
+            gvs[n % 2] = jnp.dot(both, w, preferred_element_type=F32)
 
         def gate_of(n):
             cols = slice(n * L, n * L + L)
-
-            def conv(lanes, tap):
-                return (
-                    tap[0:1, cols] * gvs[n % 2, 14:270, lanes]
-                    + tap[1:2, cols] * gvs[n % 2, 15:271, lanes]
-                    + tap[2:3, cols] * gvs[n % 2, 16:272, lanes]
-                )
-
-            cg, cv = conv(slice(0, L), gtap), conv(slice(L, 256), vtap)
-            hid[:, cols] = (cg / (1.0 + jnp.exp(-cg)) * cv).astype(BF)
+            for p in range(2):
+                at = 144 * p + 14
+
+                def conv(lanes, tap):
+                    return (
+                        tap[0:1, cols] * gvs[n % 2, at : at + 128, lanes]
+                        + tap[1:2, cols] * gvs[n % 2, at + 1 : at + 129, lanes]
+                        + tap[2:3, cols] * gvs[n % 2, at + 2 : at + 130, lanes]
+                    )
+
+                cg, cv = conv(slice(0, L), gtap), conv(slice(L, 256), vtap)
+                hid[lax.rem(i, 2), 128 * p : 128 * p + 128, cols] = (
+                    cg / (1.0 + jnp.exp(-cg)) * cv
+                ).astype(BF)
 
         product(0)
         for n in range(1, NT):
             product(n)
             gate_of(n - 1)
         gate_of(NT - 1)
-        mark('up_done')
-
-        @pl.when(i == 0)
-        def _():
-            arrived(d_far2)
-            mark('dfar2_arr')
-            for cp in d_last:
-                cp.start()
-            arrived(d_near)
-            arrived(d_last)
-            mark('dpair_arr')
-
+
+    def narrow(i):
         for n in range(8):
             w = wd[n // 2, 2 * (n % 2) : 2 * (n % 2) + 2].reshape(256, FFD)
             p = lax.dot_general(
-                hid[...], w, (((1,), (1,)), ((), ())), preferred_element_type=F32
+                hid[lax.rem(i, 2)], w, (((1,), (1,)), ((), ())), preferred_element_type=F32
             )
-            ps[slot, :, n * 256 : n * 256 + 256] = p.astype(BF)
-        mark('down_done')
-
-        @pl.when(i == 1)
+            ps[i, :, n * 256 : n * 256 + 256] = p.astype(BF)
+
+    widen(0)
+    mark('up0')
+    arrived(g1b)
+    mark('g1b_arr')
+    widen(1)
+    mark('up1')
+    arrived(d_far2)
+    mark('dfar2_arr')
+    d_pair += last_swap(wd)
+    arrived(d_pair)
+    mark('dpair_arr')
+
+    def near_down(i, _):
+        narrow(i)
+
+        @pl.when(i == 0)
         def _():
-            direct[0].start()
+            mark('down0')
+            for cp in direct:
+                cp.start()
+
+        return 0
+
+    lax.fori_loop(0, 2, near_down, 0)
+    mark('down1')
+    arrived(g2)
+    mark('g2_arr')
+
+    def rest(i, _):
+        widen(i)
+        narrow(i)
 
         @pl.when(i == 2)
         def _():
-            direct[1].start()
-
-        @pl.when(i == 3)
-        def _():
+            mark('down2')
             for cp in far:
                 cp.start()
 
         return 0
 
-    lax.fori_loop(0, 4, feed, 0)
+    lax.fori_loop(2, 4, rest, 0)
     mark('fed')
     for n, (cp, half) in enumerate(zip(far, (lo, hi))):
         cp.wait_recv()
@@ -638,8 +711,8 @@
 
         def relay(m, _):
             cols = pl.ds(pl.multiple_of(m * 256, 256), 256)
-            ps[2 * n + 1, half, cols] = (
-                ps[2 * n + 1, half, cols].astype(F32) + rl[n, :, cols].astype(F32)
+            ps[1, half, cols] = (
+                ps[1, half, cols].astype(F32) + rl[n, :, cols].astype(F32)
             ).astype(BF)
             return 0
 
@@ -652,13 +725,14 @@
 
     def add(n, _):
         cols = pl.ds(pl.multiple_of(n * 256, 256), 256)
-        s = ps[0, :, cols].astype(F32) + rr[0, :, cols].astype(F32) + rr[1, :, cols].astype(F32)
+        s = ps[3, :, cols].astype(F32) + rr[0, :, cols].astype(F32) + rr[1, :, cols].astype(F32)
         out[:, cols] = (stream[:, cols].astype(F32) + s).astype(BF)
         return 0
 
     lax.fori_loop(0, 8, add, 0)
 
     mark('added')
+    assert count['s'] <= ssem.shape[0] and count['r'] <= rsem.shape[0], count
     for cp in open_sends:
         cp.wait_send()
 
@@ -684,7 +758,7 @@
         pltpu.VMEM((1024, 256), BF), pltpu.VMEM((1024, 256), BF), pltpu.VMEM((1024, 512), BF),
         pltpu.VMEM((1024, 512), BF), pltpu.VMEM((256, D), BF),
         pltpu.VMEM((4, 4, 2, 64, 2 * FFD), BF), pltpu.VMEM((4, 4, 2, 64, FFD), BF),
-        pltpu.VMEM((4, 512, D), BF),
+        pltpu.VMEM((4, 2, 2, 4, 32, D), BF),
         pltpu.VMEM((CH, 2, DK, DV + L), F32), pltpu.VMEM((CH, 2, L, DV + L), F32),
         pltpu.VMEM((L, L), F32), pltpu.VMEM((4, 2 * CH, L), F32),
         pltpu.VMEM((CH, 2, DK, DV + L), BF), pltpu.VMEM((2, DK, DV + L), F32),
@@ -697,11 +771,11 @@
         pltpu.VMEM((DK, DV), BF), pltpu.VMEM((8, L), F32),
         pltpu.VMEM((1024, 512), BF), pltpu.VMEM((2, 128, 512), BF), pltpu.VMEM((4, 256, 512), BF),
         pltpu.VMEM((256, D), BF),
-        pltpu.VMEM((4, 272, D), BF), pltpu.VMEM((2, D), F32), pltpu.VMEM((4, 2, D), F32),
-        pltpu.VMEM((2, D), F32), pltpu.VMEM((2, 272, 256), F32), pltpu.VMEM((256, FFD), BF),
+        pltpu.VMEM((8, 144, D), BF), pltpu.VMEM((2, 2, D), F32), pltpu.VMEM((4, 2, 2, D), F32),
+        pltpu.VMEM((2, D), F32), pltpu.VMEM((2, 288, 256), F32), pltpu.VMEM((2, 256, FFD), BF),
         pltpu.VMEM((4, 256, D), BF), pltpu.VMEM((2, 128, D), BF), pltpu.VMEM((2, 256, D), BF),
-        pltpu.SemaphoreType.DMA((32,)), pltpu.SemaphoreType.DMA((100,)),
-        pltpu.SemaphoreType.DMA((100,)),
+        pltpu.SemaphoreType.DMA((32,)), pltpu.SemaphoreType.DMA((176,)),
+        pltpu.SemaphoreType.DMA((176,)),
     ]
     return pl.pallas_call(
         kernel,
@@ -715,7 +789,7 @@
     )(
         residual_entry_input, query_matrix_rows, key_matrix_rows, value_matrix_rows,
         output_gate_logits, chunks(input_gate_logits), chunks(forget_gate_logits),
-        chunks(forget_decay_offset), head_norm_gain, cell_output_weight,
+        chunks(forget_decay_offset), head_norm_gain, cell_output_weight.reshape(2, 2, 4, 32, D),
         feedforward_norm_gain.reshape(1, D), gate_up_weight, value_up_weight,
         down_projection_weight.T, gate_filter_taps, value_filter_taps,
     )

time: 142 us -> 128 us (0.901)
  Pallas kernels: 139 us -> 125 us
    pallas_call x1, Pallas kernels: 139 us -> 125 us  [local(): pl.pallas_call(kernel, out_shape=jax.ShapeDtypeStruct((256, D), BF), in_s...]
where the time goes in v3:
time: 128 us; the launch traced here: 127 us
  Pallas kernels  125 us (98%)
  local copies, waits for them, and re-layouts  2.3 us (2%)
    pallas_call x1, Pallas kernels, local(): pl.pallas_call(kernel, out_shape=jax.ShapeDtypeStruct((256, D), BF), in_s...  125 us

profile of v3, /device:TPU:0, one launch (start us, length us, event | category | flops | bytes accessed | tf_op | source)
XLA Modules:
  0.0 127.2 jit_solution(11012723554062981199)
XLA Ops:
  0.0 124.9 %shard_map.154 = bf16[256,2048]{1,0:T(8,128)(2,1)} custom-call(bf16[256,2048]{1,0:T(8,128)(2,1)} %res.1, bf16[1024,256]{1,0:T(8,128)(2,1)} %q_in.1, bf16[1024,256]{1,0:T(8,128)(2,1)} %k_in.1, bf16[1024,512]{1,0:T(8,128)(2,1)} %v_in.1, bf16[1024,512]{1,0:T(8,128)(2,1)} %og_in.1, f32[16,128]{1,0:T(8,128)} %bitcast.26, f32[16,128]{1,0:T(8,128)} %bitcast.27, ...), custom_call_target="tpu_custom_call" | custom-call | tf_op jit(solution)/shard_map/pallas_call | solution.py:780
  124.9 2.3 %copy.21 = bf16[256,2048]{1,0:T(8,128)(2,1)} copy(bf16[256,2048]{1,0:T(8,128)(2,1)} %shard_map.154) | data formatting | bytes 2097152

commit v4 on v3

--- a/solution.py
+++ b/solution.py
@@ -11,6 +11,7 @@
 MESH = pl.DeviceIdType.MESH
 
 EPS = 1e-06
+FIRST = 0
 NEG = -1e30
 L = 128
 CH = 8
@@ -34,7 +35,7 @@
     out,
     q, k, v, og, rsd, wgv, wd, wo, dc, nl, colt, rows, cs, cpri, mpri, rs_rows,
     st1, ax1, st1r, ax1r, st2, ax2, st3, ax3, st4, ax4, st4r, ax4r,
-    gated, al, orr, stream, gr, hs, hr, hp, gvs, hid, ps, rl, rr,
+    gated, al, orr, stream, gr, hs, hl, hp, gvs, hid, ps, rl, rr,
     lsem, ssem, rsem,
 ):
     z, y, c, tp = (lax.axis_index(a) for a in SP_TP)
@@ -177,16 +178,6 @@
         row_a = ref.at[z, :, c, pl.ds(0, 32)]
         row_b = ref.at[:, y, c, pl.ds(32, 32)]
         return [send(row_a, row_a, {"sp_2": other}), send(row_b, row_b, {"sp_2": other})]
-
-    def across(ref):
-        row_a = ref.at[z, :, c, pl.ds(0, 32)]
-        row_b = ref.at[:, y, c, pl.ds(32, 32)]
-        return [
-            send(row_a, row_a, {"sp_0": z1}),
-            send(row_a, row_a, {"sp_0": z3}),
-            send(row_b, row_b, {"sp_1": y1}),
-            send(row_b, row_b, {"sp_1": y3}),
-        ]
 
     def across_two(ref):
         far = [
@@ -458,38 +449,45 @@
             gated[at, h * DV : (h + 1) * DV] = (mo * norm * gain[h : h + 1, :] * gate).astype(BF)
         return 0
 
-    a2a = []
-    for n in (2, 1, 3, 0):
-        b = up(tp, n)
-        lax.fori_loop(2 * b, 2 * b + 2, finish, 0)
-        block = pl.ds(pl.multiple_of(b * 256, 256), 256)
-        half0 = pl.ds(pl.multiple_of(b * 256, 128), 128)
-        half1 = pl.ds(pl.multiple_of(b * 256 + 128, 128), 128)
-        if n == 2:
-            first_leg = [
-                send(gated.at[half0], al.at[0], {"tp": x1}),
-                send(gated.at[half1], al.at[1], {"tp": x3}),
-            ]
-        elif n:
-            a2a.append(send(gated.at[block], orr.at[tp], {"tp": b}))
-        else:
-            orr[tp] = gated[block, :]
-        if n == 1:
-            mark('cell_two')
+    a2a, legs, relayed = [[], []], [None, None], [None, None]
+
+    def pass_on(half):
+        arrived(legs[half])
+        relayed[half] = [
+            send(al.at[half, 0], orr.at[x3, pl.ds(128 * half, 64)], {"tp": x1}),
+            send(al.at[half, 1], orr.at[x1, pl.ds(128 * half + 64, 64)], {"tp": x3}),
+        ]
+
+    for half in (0, 1):
+        for n in (2, 1, 3, 0):
+            j = 2 * up(tp, n) + half
+            lax.fori_loop(j, j + 1, finish, 0)
+            start = pl.multiple_of(j * L, L)
+            place_of = pl.ds(128 * half, 128)
+            if n == 2:
+                legs[half] = [
+                    send(gated.at[pl.ds(start, 64)], al.at[half, 0], {"tp": x1}),
+                    send(gated.at[pl.ds(start + 64, 64)], al.at[half, 1], {"tp": x3}),
+                ]
+                if half:
+                    mark('cell_hi2')
+                    pass_on(0)
+                    mark('leg0_arr')
+            elif n:
+                a2a[half].append(
+                    send(gated.at[pl.ds(start, 128)], orr.at[tp, place_of], {"tp": up(tp, n)})
+                )
+            else:
+                orr[tp, place_of] = gated[pl.ds(start, 128), :]
+        if not half:
+            mark('cell_lo')
             arrived(near_a)
             arrived(near_b)
             mark('near_ab')
             wpair += wo_near_swaps(x1) + wo_near_swaps(x3)
             for t in (x1, x3):
                 wpair += [wo_swap(piece) for piece in wo_pieces(t, True)]
-        if n == 3:
-            mark('cell_three')
-            arrived(first_leg)
-            mark('leg_arr')
-            relayed = [
-                send(al.at[0], orr.at[x3, pl.ds(0, 128)], {"tp": x1}),
-                send(al.at[1], orr.at[x1, pl.ds(128, 128)], {"tp": x3}),
-            ]
+    pass_on(1)
     mark('cell_done')
     arrived(near_c)
     mark('near_c')
@@ -499,79 +497,80 @@
     mark('p2_arr')
     g_far1 += slab(wgv, 2)
     g_pair = row_swap(wgv)
+    d_far1 = slab(wd, 0)
 
     mark('w2_arr')
-    arrived(relayed)
-    arrived(a2a)
-    mark('a2a_arr')
-    arrived(wpair)
-    mark('wpair_arr')
     ld_res.wait()
 
-    def project(n, ss):
-        cols = pl.ds(pl.multiple_of(n * 256, 256), 256)
-        acc = rsd[:, cols].astype(F32)
-        for t in range(4):
-            acc = acc + jnp.dot(orr[t], wo[t, :, :, :, :, cols].reshape(512, 256), preferred_element_type=F32)
-        low = acc.astype(BF)
-        stream[:, cols] = low
-        wide = low.astype(F32)
-        sq = wide * wide
-        return ss + sq[:, :L] + sq[:, L:]
-
-    ss = lax.fori_loop(0, 8, project, jnp.zeros((256, L), F32))
-    mark('projected')
-    norm = lax.rsqrt(jnp.sum(ss, axis=1, keepdims=True) * (1.0 / D) + EPS)
-
-    def normed(n, _):
-        cols = pl.ds(pl.multiple_of(n * 256, 256), 256)
-        rows_n = (stream[:, cols].astype(F32) * norm * fgain[:, cols]).astype(BF)
-        gr[2 * tp, pl.ds(16, 128), cols] = rows_n[:128]
-        gr[2 * tp + 1, pl.ds(16, 128), cols] = rows_n[128:]
-        hs[0, :, cols] = rows_n[254:256].astype(F32)
-        hs[1, :, cols] = rows_n[126:128].astype(F32)
-        return 0
-
-    lax.fori_loop(0, 8, normed, 0)
-
-    mark('normed')
-    hr[tp] = hs[...]
+    def half_rows(b, h):
+        return gr.at[2 * b + h, pl.ds(16, 128)]
+
+    gather = [None, None]
+    for half in (0, 1):
+        at = slice(128 * half, 128 * half + 128)
+        arrived(relayed[half] + a2a[half])
+        mark('a2a_arr')
+        if not half:
+            arrived(wpair)
+            mark('wpair_arr')
+
+        def project(n, ss):
+            cols = pl.ds(pl.multiple_of(n * 256, 256), 256)
+            acc = rsd[at, cols].astype(F32)
+            for t in range(4):
+                acc = acc + jnp.dot(
+                    orr[t, at], wo[t, :, :, :, :, cols].reshape(512, 256),
+                    preferred_element_type=F32,
+                )
+            low = acc.astype(BF)
+            stream[at, cols] = low
+            wide = low.astype(F32)
+            sq = wide * wide
+            return ss + sq[:, :L] + sq[:, L:]
+
+        ss = lax.fori_loop(0, 8, project, jnp.zeros((128, L), F32))
+        norm = lax.rsqrt(jnp.sum(ss, axis=1, keepdims=True) * (1.0 / D) + EPS)
+
+        def normed(n, _):
+            cols = pl.ds(pl.multiple_of(n * 256, 256), 256)
+            rows_n = (stream[at, cols].astype(F32) * norm * fgain[:, cols]).astype(BF)
+            gr[2 * tp + half, pl.ds(16, 128), cols] = rows_n
+            if half:
+                hs[:, cols] = rows_n[126:128].astype(F32)
+            return 0
+
+        lax.fori_loop(0, 8, normed, 0)
+        mark('normed')
+        mine = half_rows(tp, half)
+        gather[half] = [send(mine, mine, {"tp": x1}), send(mine, mine, {"tp": x3})]
+
+    halo = send(hs, hl, {"tp": x2})
     s_next = [take("s") for _ in range(4)]
     r_next = take("r")
 
     def next_copy(t):
         return pltpu.make_async_remote_copy(
-            src_ref=hs.at[0], dst_ref=hp, send_sem=ssem.at[s_next[t]], recv_sem=rsem.at[r_next],
+            src_ref=hs, dst_ref=hp, send_sem=ssem.at[s_next[t]], recv_sem=rsem.at[r_next],
             device_id={**at_place(place + 1), "tp": t}, device_id_type=MESH,
         )
 
-    def half_rows(b, h):
-        return gr.at[2 * b + h, pl.ds(16, 128)]
-
-    own_lo, own_hi = half_rows(tp, 0), half_rows(tp, 1)
-    g1a = [send(own_lo, own_lo, {"tp": x1}), send(own_hi, own_hi, {"tp": x3})]
-    halo = [send(hs, hr.at[tp], {"tp": up(tp, n)}) for n in (1, 2, 3)]
     @pl.when(tp == 3)
     def _():
         for t in range(4):
             next_copy(t).start()
-
-    g1b = [send(own_hi, own_hi, {"tp": x1}), send(own_lo, own_lo, {"tp": x3})]
 
     mark('g1_sent')
     arrived(g_far1)
     mark('gfar1_arr')
     g_far2, more = across_two(wgv)
     g_pair += more
-    d_far1 = across(wd)
+    for n in (1, 3, 2):
+        d_far1 += slab(wd, n)
     d_pair = row_swap(wd)
-    arrived(halo)
-    next_copy(0).wait_recv()
-    mark('halo_arr')
-    arrived(g1a)
+    arrived(gather[0])
     mark('g1a_arr')
-    part_a, part_b = half_rows(x3, 0), half_rows(x1, 1)
-    g2 = [send(part_a, part_a, {"tp": x1}), send(part_b, part_b, {"tp": x3})]
+    part_a = half_rows(x3, 0)
+    g2 = [send(part_a, part_a, {"tp": x1})]
     arrived(g_far2)
     mark('gfar2_arr')
     g_pair += last_swap(wgv)
@@ -579,10 +578,20 @@
     mark('dfar1_arr')
     d_far2, more = across_two(wd)
     d_pair += more
+    arrived(gather[1])
+    mark('g1b_arr')
+    part_b = half_rows(x1, 1)
+    g2.append(send(part_b, part_b, {"tp": x3}))
+    arrived([halo])
+    next_copy(0).wait_recv()
+    mark('halo_arr')
     arrived(g_pair)
     mark('gpair_arr')
 
-    first = jnp.full((2, D), place, jnp.int32) == 0
+    def tail_of(two):
+        return jnp.concatenate([jnp.zeros((14, D), F32), two], axis=0)
+
+    from_before = tail_of(jnp.where(jnp.full((2, D), place, jnp.int32) == 0, 0.0, hp[...]))
 
     def copy_of(src, dst, dev):
         cp = pltpu.make_async_remote_copy(
@@ -615,16 +624,13 @@
 
     def widen(i):
         spots = rows_of(i)
-        for b, h in spots:
-            from_last = jnp.where(
-                jnp.full((2, D), b, jnp.int32) == 0,
-                jnp.where(first, 0.0, hp[...]),
-                hr[up(b, 3), 0],
-            )
-            two = jnp.where(jnp.full((2, D), h, jnp.int32) == 1, hr[b, 1], from_last)
-            gr[2 * b + h, pl.ds(0, 16), :] = jnp.concatenate(
-                [jnp.zeros((14, D), F32), two], axis=0
-            ).astype(BF)
+        for m, (b, h) in enumerate(spots):
+            if i is FIRST and m:
+                near = tail_of(hl[...])
+            else:
+                near = gr[2 * up(b, 3 + h) + 1 - h, pl.ds(128, 16), :].astype(F32)
+            starts = jnp.full((16, D), b + 4 * h, jnp.int32) == 0
+            gr[2 * b + h, pl.ds(0, 16), :] = jnp.where(starts, from_before, near).astype(BF)
         e0, e1 = (2 * b + h for b, h in spots)
 
         def product(n):
@@ -663,30 +669,19 @@
             )
             ps[i, :, n * 256 : n * 256 + 256] = p.astype(BF)
 
-    widen(0)
+    widen(FIRST)
     mark('up0')
-    arrived(g1b)
-    mark('g1b_arr')
-    widen(1)
-    mark('up1')
     arrived(d_far2)
     mark('dfar2_arr')
     d_pair += last_swap(wd)
     arrived(d_pair)
     mark('dpair_arr')
-
-    def near_down(i, _):
-        narrow(i)
-
-        @pl.when(i == 0)
-        def _():
-            mark('down0')
-            for cp in direct:
-                cp.start()
-
-        return 0
-
-    lax.fori_loop(0, 2, near_down, 0)
+    narrow(FIRST)
+    mark('down0')
+    for cp in direct:
+        cp.start()
+    widen(1)
+    narrow(1)
     mark('down1')
     arrived(g2)
     mark('g2_arr')
@@ -769,9 +764,9 @@
         pltpu.VMEM((4, DK, DV), BF), pltpu.VMEM((4, 8, L), F32),
         pltpu.VMEM((DK, DV), BF), pltpu.VMEM((8, L), F32),
         pltpu.VMEM((DK, DV), BF), pltpu.VMEM((8, L), F32),
-        pltpu.VMEM((1024, 512), BF), pltpu.VMEM((2, 128, 512), BF), pltpu.VMEM((4, 256, 512), BF),
+        pltpu.VMEM((1024, 512), BF), pltpu.VMEM((2, 2, 64, 512), BF), pltpu.VMEM((4, 256, 512), BF),
         pltpu.VMEM((256, D), BF),
-        pltpu.VMEM((8, 144, D), BF), pltpu.VMEM((2, 2, D), F32), pltpu.VMEM((4, 2, 2, D), F32),
+        pltpu.VMEM((8, 144, D), BF), pltpu.VMEM((2, D), F32), pltpu.VMEM((2, D), F32),
         pltpu.VMEM((2, D), F32), pltpu.VMEM((2, 288, 256), F32), pltpu.VMEM((2, 256, FFD), BF),
         pltpu.VMEM((4, 256, D), BF), pltpu.VMEM((2, 128, D), BF), pltpu.VMEM((2, 256, D), BF),
         pltpu.SemaphoreType.DMA((32,)), pltpu.SemaphoreType.DMA((176,)),

time: 128 us -> 123 us (0.961)
  Pallas kernels: 125 us -> 120 us
    pallas_call x1, Pallas kernels: 125 us -> 120 us  [local(): pl.pallas_call(kernel, out_shape=jax.ShapeDtypeStruct((256, D), BF), in_s...]
where the time goes in v4:
time: 123 us; the launch traced here: 122 us
  Pallas kernels  120 us (98%)
  local copies, waits for them, and re-layouts  2.3 us (2%)
    pallas_call x1, Pallas kernels, local(): pl.pallas_call(kernel, out_shape=jax.ShapeDtypeStruct((256, D), BF), in_s...  120 us

profile of v4, /device:TPU:0, one launch (start us, length us, event | category | flops | bytes accessed | tf_op | source)
XLA Modules:
  0.0 122.2 jit_solution(4956752508389203007)
XLA Ops:
  0.0 119.9 %shard_map.154 = bf16[256,2048]{1,0:T(8,128)(2,1)} custom-call(bf16[256,2048]{1,0:T(8,128)(2,1)} %res.1, bf16[1024,256]{1,0:T(8,128)(2,1)} %q_in.1, bf16[1024,256]{1,0:T(8,128)(2,1)} %k_in.1, bf16[1024,512]{1,0:T(8,128)(2,1)} %v_in.1, bf16[1024,512]{1,0:T(8,128)(2,1)} %og_in.1, f32[16,128]{1,0:T(8,128)} %bitcast.26, f32[16,128]{1,0:T(8,128)} %bitcast.27, ...), custom_call_target="tpu_custom_call" | custom-call | tf_op jit(solution)/shard_map/pallas_call | solution.py:775
  119.9 2.3 %copy.21 = bf16[256,2048]{1,0:T(8,128)(2,1)} copy(bf16[256,2048]{1,0:T(8,128)(2,1)} %shard_map.154) | data formatting | bytes 2097152

commit v5 on v4

--- a/solution.py
+++ b/solution.py
@@ -505,6 +505,15 @@
     def half_rows(b, h):
         return gr.at[2 * b + h, pl.ds(16, 128)]
 
+    s_next = [take("s") for _ in range(4)]
+    r_next = take("r")
+
+    def next_copy(t):
+        return pltpu.make_async_remote_copy(
+            src_ref=hs, dst_ref=hp, send_sem=ssem.at[s_next[t]], recv_sem=rsem.at[r_next],
+            device_id={**at_place(place + 1), "tp": t}, device_id_type=MESH,
+        )
+
     gather = [None, None]
     for half in (0, 1):
         at = slice(128 * half, 128 * half + 128)
@@ -541,23 +550,16 @@
 
         lax.fori_loop(0, 8, normed, 0)
         mark('normed')
+        if half:
+            halo = send(hs, hl, {"tp": x2})
+
+            @pl.when(tp == 3)
+            def _():
+                for t in range(4):
+                    next_copy(t).start()
+
         mine = half_rows(tp, half)
         gather[half] = [send(mine, mine, {"tp": x1}), send(mine, mine, {"tp": x3})]
-
-    halo = send(hs, hl, {"tp": x2})
-    s_next = [take("s") for _ in range(4)]
-    r_next = take("r")
-
-    def next_copy(t):
-        return pltpu.make_async_remote_copy(
-            src_ref=hs, dst_ref=hp, send_sem=ssem.at[s_next[t]], recv_sem=rsem.at[r_next],
-            device_id={**at_place(place + 1), "tp": t}, device_id_type=MESH,
-        )
-
-    @pl.when(tp == 3)
-    def _():
-        for t in range(4):
-            next_copy(t).start()
 
     mark('g1_sent')
     arrived(g_far1)
@@ -602,17 +604,27 @@
         return cp
 
     lo, hi = pl.ds(0, 128), pl.ds(128, 128)
+    col_halves = (pl.ds(0, 1024), pl.ds(1024, 1024))
     direct = [
-        copy_of(ps.at[0, lo], rr.at[0, hi], {"tp": x1}),
-        copy_of(ps.at[0, hi], rr.at[1, lo], {"tp": x3}),
+        (
+            copy_of(ps.at[0, lo, q], rr.at[0, hi, q], {"tp": x1}),
+            copy_of(ps.at[0, hi, q], rr.at[1, lo, q], {"tp": x3}),
+        )
+        for q in col_halves
     ]
     far = [
-        copy_of(ps.at[2, lo], rl.at[0], {"tp": x1}),
-        copy_of(ps.at[2, hi], rl.at[1], {"tp": x3}),
+        (
+            copy_of(ps.at[2, lo, q], rl.at[0, :, q], {"tp": x1}),
+            copy_of(ps.at[2, hi, q], rl.at[1, :, q], {"tp": x3}),
+        )
+        for q in col_halves
     ]
     summed = [
-        copy_of(ps.at[1, lo], rr.at[0, lo], {"tp": x1}),
-        copy_of(ps.at[1, hi], rr.at[1, hi], {"tp": x3}),
+        (
+            copy_of(ps.at[1, lo, q], rr.at[0, lo, q], {"tp": x1}),
+            copy_of(ps.at[1, hi, q], rr.at[1, hi, q], {"tp": x3}),
+        )
+        for q in col_halves
     ]
 
     def rows_of(i):
@@ -661,13 +673,15 @@
             gate_of(n - 1)
         gate_of(NT - 1)
 
-    def narrow(i):
+    def narrow(i, leave=None):
         for n in range(8):
             w = wd[n // 2, 2 * (n % 2) : 2 * (n % 2) + 2].reshape(256, FFD)
             p = lax.dot_general(
                 hid[lax.rem(i, 2)], w, (((1,), (1,)), ((), ())), preferred_element_type=F32
             )
             ps[i, :, n * 256 : n * 256 + 256] = p.astype(BF)
+            if leave and n % 4 == 3:
+                leave(n // 4)
 
     widen(FIRST)
     mark('up0')
@@ -676,47 +690,43 @@
     d_pair += last_swap(wd)
     arrived(d_pair)
     mark('dpair_arr')
-    narrow(FIRST)
+
+    def start_direct(m):
+        for cp in direct[m]:
+            cp.start()
+
+    narrow(FIRST, start_direct)
     mark('down0')
-    for cp in direct:
-        cp.start()
     widen(1)
     narrow(1)
     mark('down1')
     arrived(g2)
     mark('g2_arr')
 
-    def rest(i, _):
-        widen(i)
-        narrow(i)
-
-        @pl.when(i == 2)
-        def _():
-            mark('down2')
-            for cp in far:
-                cp.start()
-
-        return 0
-
-    lax.fori_loop(2, 4, rest, 0)
+    def start_far(m):
+        for cp in far[m]:
+            cp.start()
+
+    widen(2)
+    narrow(2, start_far)
+    mark('down2')
+    widen(3)
+    narrow(3)
     mark('fed')
-    for n, (cp, half) in enumerate(zip(far, (lo, hi))):
-        cp.wait_recv()
-        mark('far_arr')
-
-        def relay(m, _):
-            cols = pl.ds(pl.multiple_of(m * 256, 256), 256)
-            ps[1, half, cols] = (
-                ps[1, half, cols].astype(F32) + rl[n, :, cols].astype(F32)
-            ).astype(BF)
-            return 0
-
-        lax.fori_loop(0, 8, relay, 0)
-        summed[n].start()
-    arrived(direct)
-    mark('direct_arr')
-    arrived(summed)
-    mark('back_arr')
+    for m in (0, 1):
+        for n, half in enumerate((lo, hi)):
+            far[m][n].wait_recv()
+            mark('far_arr')
+
+            def relay(t, _):
+                cols = pl.ds(pl.multiple_of(t * 256, 256), 256)
+                ps[1, half, cols] = (
+                    ps[1, half, cols].astype(F32) + rl[n, :, cols].astype(F32)
+                ).astype(BF)
+                return 0
+
+            lax.fori_loop(4 * m, 4 * m + 4, relay, 0)
+            summed[m][n].start()
 
     def add(n, _):
         cols = pl.ds(pl.multiple_of(n * 256, 256), 256)
@@ -724,7 +734,10 @@
         out[:, cols] = (stream[:, cols].astype(F32) + s).astype(BF)
         return 0
 
-    lax.fori_loop(0, 8, add, 0)
+    for m in (0, 1):
+        arrived(direct[m] + summed[m])
+        mark('back_arr')
+        lax.fori_loop(4 * m, 4 * m + 4, add, 0)
 
     mark('added')
     assert count['s'] <= ssem.shape[0] and count['r'] <= rsem.shape[0], count

time: 123 us -> 120 us (0.976)
  Pallas kernels: 120 us -> 118 us
    pallas_call x1, Pallas kernels: 120 us -> 118 us  [local(): pl.pallas_call(kernel, out_shape=jax.ShapeDtypeStruct((256, D), BF), in_s...]
where the time goes in v5:
time: 120 us
  Pallas kernels  118 us (98%)
  local copies, waits for them, and re-layouts  2.3 us (2%)
    pallas_call x1, Pallas kernels, local(): pl.pallas_call(kernel, out_shape=jax.ShapeDtypeStruct((256, D), BF), in_s...  118 us

profile of v5, /device:TPU:0, one launch (start us, length us, event | category | flops | bytes accessed | tf_op | source)
XLA Modules:
  0.0 120.1 jit_solution(17605596076619010023)
XLA Ops:
  0.0 117.8 %shard_map.154 = bf16[256,2048]{1,0:T(8,128)(2,1)} custom-call(bf16[256,2048]{1,0:T(8,128)(2,1)} %res.1, bf16[1024,256]{1,0:T(8,128)(2,1)} %q_in.1, bf16[1024,256]{1,0:T(8,128)(2,1)} %k_in.1, bf16[1024,512]{1,0:T(8,128)(2,1)} %v_in.1, bf16[1024,512]{1,0:T(8,128)(2,1)} %og_in.1, f32[16,128]{1,0:T(8,128)} %bitcast.26, f32[16,128]{1,0:T(8,128)} %bitcast.27, ...), custom_call_target="tpu_custom_call" | custom-call | tf_op jit(solution)/shard_map/pallas_call | solution.py:788
  117.8 2.3 %copy.21 = bf16[256,2048]{1,0:T(8,128)(2,1)} copy(bf16[256,2048]{1,0:T(8,128)(2,1)} %shard_map.154) | data formatting | bytes 2097152

commit v6 on v5

--- a/solution.py
+++ b/solution.py
@@ -571,8 +571,13 @@
     d_pair = row_swap(wd)
     arrived(gather[0])
     mark('g1a_arr')
-    part_a = half_rows(x3, 0)
-    g2 = [send(part_a, part_a, {"tp": x1})]
+
+    def onward(h):
+        part_a = gr.at[2 * x3 + h, pl.ds(16, 64)]
+        part_b = gr.at[2 * x1 + h, pl.ds(80, 64)]
+        return [send(part_a, part_a, {"tp": x1}), send(part_b, part_b, {"tp": x3})]
+
+    g2 = onward(0)
     arrived(g_far2)
     mark('gfar2_arr')
     g_pair += last_swap(wgv)
@@ -582,8 +587,7 @@
     d_pair += more
     arrived(gather[1])
     mark('g1b_arr')
-    part_b = half_rows(x1, 1)
-    g2.append(send(part_b, part_b, {"tp": x3}))
+    g2 += onward(1)
     arrived([halo])
     next_copy(0).wait_recv()
     mark('halo_arr')

time: 120 us -> 120 us (level); the launches traced: 120 us -> 117 us
  Pallas kernels: 118 us -> 115 us
    pallas_call x1, Pallas kernels: 118 us -> 115 us  [local(): pl.pallas_call(kernel, out_shape=jax.ShapeDtypeStruct((256, D), BF), in_s...]
where the time goes in v6:
time: 120 us; the launch traced here: 117 us
  Pallas kernels  115 us (96%)
  local copies, waits for them, and re-layouts  2.3 us (2%)
    pallas_call x1, Pallas kernels, local(): pl.pallas_call(kernel, out_shape=jax.ShapeDtypeStruct((256, D), BF), in_s...  115 us

profile of v6, /device:TPU:0, one launch (start us, length us, event | category | flops | bytes accessed | tf_op | source)
XLA Modules:
  0.0 117.4 jit_solution(6779390475303302022)
XLA Ops:
  0.0 115.1 %shard_map.154 = bf16[256,2048]{1,0:T(8,128)(2,1)} custom-call(bf16[256,2048]{1,0:T(8,128)(2,1)} %res.1, bf16[1024,256]{1,0:T(8,128)(2,1)} %q_in.1, bf16[1024,256]{1,0:T(8,128)(2,1)} %k_in.1, bf16[1024,512]{1,0:T(8,128)(2,1)} %v_in.1, bf16[1024,512]{1,0:T(8,128)(2,1)} %og_in.1, f32[16,128]{1,0:T(8,128)} %bitcast.26, f32[16,128]{1,0:T(8,128)} %bitcast.27, ...), custom_call_target="tpu_custom_call" | custom-call | tf_op jit(solution)/shard_map/pallas_call | solution.py:792
  115.1 2.3 %copy.21 = bf16[256,2048]{1,0:T(8,128)(2,1)} copy(bf16[256,2048]{1,0:T(8,128)(2,1)} %shard_map.154) | data formatting | bytes 2097152
